TPU v7x, 128 devices: a whole 4x4x4 slice. The times are simulated.
128 devices in a mesh: fs: 16 (over z, y), tp: 8 (over x, core).
Axes of the slice: x: 4, y: 4, z: 4, core: 2. Of those that a mesh axis runs over, the one named last changes fastest.
Arguments:
- prompt: bfloat16 [8192, 4096], P('fs'), may hold values from -6 to 6
- expert_ids: int32 [8192, 2], P('fs'), may hold values from 0 to 31, all different within a row; in each aligned block of 512 rows (0 to 511, 512 to 1023, ...) at most 48 rows name the same one
- group_weight: float32 [8192], P('fs'), may hold values from 0.25 to 1
- expert_share: float32 [8192, 2], P('fs'), may hold values from 0.1 to 1
- norm_gain: float32 [4096], P('fs'), may hold values from 0.1 to 1.9
- gate_train: float32 [32, 4096, 1024], P(None, 'fs', 'tp'), may hold values from -0.09375 to 0.09375
- up_train: float32 [32, 4096, 1024], P(None, 'fs', 'tp'), may hold values from -0.09375 to 0.09375
- down_train: float32 [32, 1024, 4096], P(None, 'fs', 'tp'), may hold values from -0.1875 to 0.1875
Outputs:
- mixed: bfloat16 [8192, 4096], P('fs', 'tp')
- gate_new: bfloat16 [32, 4096, 1024], P('fs', None, 'tp')
- up_new: bfloat16 [32, 4096, 1024], P('fs', None, 'tp')
- down_new: bfloat16 [32, 1024, 4096], P('fs', 'tp')
Inputs may be any that keep to these rules, and one draw needn't show every extreme that they name: `expert_ids`: each row names two different experts; within the rows of one index of fs no expert is named more than 48 times, a bound that some block reaches there.
All inputs are finite; a program needn't handle non-finite values.
Results may differ from a plain program's by a relative error of at most 0.0086.
Values may be sent and summed in bfloat16 or wider, within the bound.
A program may use at most 128 MiB of HBM per device.

v0:
```python
import jax
import jax.numpy as jnp
from jax import lax
from jax.sharding import PartitionSpec as P

EPS = 1e-06


def side_by_side(arrays, axis, split_dim, concat_dim, along):
    widths = [a.shape[along] for a in arrays]
    both = jnp.concatenate(arrays, axis=along)
    filled = lax.all_to_all(both, axis, split_axis=split_dim, concat_axis=concat_dim, tiled=True)
    return tuple(jnp.split(filled, [sum(widths[:k]) for k in range(1, len(widths))], axis=along))


def on_device(
    prompt, expert_ids, group_weight, expert_share, norm_gain, gate_train, up_train, down_train
):
    gain_rows = norm_gain[None, :, None]
    gate_cast = (gate_train * gain_rows).astype(jnp.bfloat16)
    up_cast = (up_train * gain_rows).astype(jnp.bfloat16)
    gate_new, up_new = side_by_side((gate_cast, up_cast), "fs", 0, 1, 2)
    down_cols = lax.all_to_all(
        down_train.astype(jnp.bfloat16), "fs", split_axis=0, concat_axis=1, tiled=True
    )
    down_new = lax.all_to_all(down_cols, "tp", split_axis=1, concat_axis=2, tiled=True)
    fs_count = lax.axis_size("fs")
    tp_count = lax.axis_size("tp")
    tokens, model_width = prompt.shape
    experts_all = gate_train.shape[0]
    local_experts = gate_new.shape[0]
    capacity = max(2, 3 * tokens // experts_all)
    widened = prompt.astype(jnp.float32)
    normed = (
        widened * lax.rsqrt(jnp.mean(widened * widened, axis=-1, keepdims=True) + EPS)
    ).astype(jnp.bfloat16)
    flat_ids = expert_ids.reshape(-1)
    onehot = (flat_ids[:, None] == jnp.arange(experts_all, dtype=jnp.int32)[None, :]).astype(
        jnp.int32
    )
    slot_rank = jnp.sum((jnp.cumsum(onehot, axis=0) - 1) * onehot, axis=1)
    targets = (flat_ids * capacity + slot_rank).reshape(tokens, 2)
    slot_ids = jnp.arange(experts_all * capacity, dtype=jnp.int32)
    picker = jnp.sum((targets[None, :, :] == slot_ids[:, None, None]).astype(jnp.bfloat16), axis=2)
    slice_width = model_width // tp_count
    own_columns = lax.dynamic_slice_in_dim(
        normed, lax.axis_index("tp") * slice_width, slice_width, 1
    )
    outgoing = jnp.dot(picker, own_columns, preferred_element_type=jnp.float32).astype(jnp.bfloat16)
    arrived = lax.all_to_all(
        outgoing.reshape(fs_count, local_experts, capacity, own_columns.shape[1]),
        "fs",
        split_axis=0,
        concat_axis=2,
        tiled=True,
    )[0]
    piece = lax.all_gather(arrived, "tp", axis=2, tiled=True)
    gate_val = jnp.einsum("erd,edf->erf", piece, gate_new, preferred_element_type=jnp.float32)
    up_val = jnp.einsum("erd,edf->erf", piece, up_new, preferred_element_type=jnp.float32)
    hidden = (jax.nn.silu(gate_val) * up_val).astype(jnp.bfloat16)
    own_width = model_width // tp_count
    summed_rows = jnp.einsum(
        "erf,efc->erc",
        lax.all_gather(hidden, "tp", axis=2, tiled=True),
        down_cols,
        preferred_element_type=jnp.float32,
    )
    summed = jnp.transpose(summed_rows, (2, 0, 1)).reshape(own_width, -1)
    outgoing_back = summed.astype(jnp.bfloat16).reshape(
        own_width, local_experts, fs_count, capacity
    )
    returned = lax.all_to_all(outgoing_back, "fs", split_axis=2, concat_axis=1, tiled=True)
    returned_rows = returned.reshape(own_width, experts_all * capacity)
    picked = jnp.take(returned_rows, targets, axis=1).astype(jnp.float32)
    weights = group_weight[:, None] * expert_share / jnp.sum(expert_share, axis=1, keepdims=True)
    mixed = jnp.sum(picked * weights[None, :, :], axis=2)
    return (mixed.T.astype(jnp.bfloat16), gate_new, up_new, down_new)


def solution(mesh):
    placed = (
        P("fs", None),
        P("fs", None),
        P("fs"),
        P("fs", None),
        P("fs"),
        P(None, "fs", "tp"),
        P(None, "fs", "tp"),
        P(None, "fs", "tp"),
    )
    return jax.shard_map(
        on_device,
        mesh=mesh,
        in_specs=placed,
        out_specs=(P("fs", "tp"), P("fs", None, "tp"), P("fs", None, "tp"), P("fs", "tp", None)),
        check_vma=False,
    )
```

profile of v0, /device:TPU:1, one launch (start us, length us, event | category | flops | bytes accessed | tf_op | source)
XLA Modules:
  0.0 258.7 jit_solution(8319599515757165364)
XLA Ops:
  8.4 6.6 %convert_element_type.52 = f32[512,4096]{1,0:T(8,128)} convert(bf16[512,4096]{1,0:T(8,128)(2,1)} %param.8) | non-fusion elementwise | flops 2097152 | bytes 12582912 | tf_op jit(solution)/shard_map/convert_element_type | solution.py:33
  16.0 9.0 %reduce-window.6 = s32[32,8,128]{2,1,0:T(8,128)S(1)} reduce-window(s32[32,8,128]{2,1,0:T(8,128)S(1)} %fusion.8, s32[]{:T(128)} %constant.17.clone.1), window={size=1x1x128 pad=0_0x0_0x127_0}, to_apply=%region_0.0 | reduce-window | flops 4161536 | bytes 262148 | tf_op jit(solution)/shard_map/reduce-window
  25.8 1.5 fusion.1
  27.3 2.3 convolution_convert_fusion
  29.6 30.0 %all_to_all.84 = bf16[16,2,48,512]{3,2,1,0:T(8,128)(2,1)S(1)} all-to-all(bf16[16,2,48,512]{3,2,1,0:T(8,128)(2,1)S(1)} %bitcast.56), channel_id=1, replica_groups=mesh['fs'=16,'tp'=8] {'fs'}, dimensions={0} | all-to-all | bytes 3145728 | tf_op jit(solution)/shard_map/all_to_all | solution.py:50
  61.0 4.6 %multiply_convert_fusion.1 = (bf16[32,256,128]{2,1,0:T(8,128)(2,1)S(1)}, bf16[32,256,128]{2,1,0:T(8,128)(2,1)S(1)}) fusion(f32[32,256,128]{2,1,0:T(8,128)} %param.13, f32[256]{0:T(256)S(1)} %copy-done.10, f32[32,256,128]{2,1,0:T(8,128)} %param.14), kind=kLoop, calls=%fused_computation.6 | loop fusion | flops 4194304 | bytes 12583936 | tf_op jit(solution)/shard_map/convert_element_type | solution.py:20
  66.2 53.1 %all_to_all.85 = bf16[32,256,256]{2,1,0:T(8,128)(2,1)S(1)} all-to-all(bf16[32,256,256]{2,1,0:T(8,128)(2,1)S(1)} %pad_maximum_fusion), channel_id=1, replica_groups=mesh['fs'=16,'tp'=8] {'fs'}, dimensions={0} | all-to-all | bytes 8388608 | tf_op jit(solution)/shard_map/all_to_all | solution.py:12
  119.7 2.0 fusion.10
  121.7 5.9 %all-gather.3.cloned.1.call-done = bf16[2,768,4096]{2,1,0:T(8,128)(2,1)} async-done(((bf16[2,768,512]{2,1,0:T(8,128)(2,1)}), bf16[2,768,4096]{2,1,0:T(8,128)(2,1)}) %all-gather.3.cloned.1.call-update) | async-done | bytes 12582928 | tf_op jit(solution)/shard_map/all_gather | solution.py:57
  127.6 6.6 %fusion.11 = f32[2,768,128]{2,1,0:T(8,128)S(1)} fusion(bf16[2,768,4096]{2,1,0:T(8,128)(2,1)} %all-gather.3.cloned.1.call-done, bf16[2,4096,128]{2,1,0:T(8,128)(2,1)S(1)} %get-tuple-element.6), kind=kOutput, calls=%fused_computation.32 | convolution fusion | flops 1610612736 | bytes 15466496 | tf_op jit(solution)/shard_map/erd,edf->erf/dot_general | solution.py:58
  134.2 2.2 copy-done.11
  136.5 4.2 %fusion.2 = bf16[2,768,128]{2,1,0:T(8,128)(2,1)} fusion(bf16[2,768,4096]{2,1,0:T(8,128)(2,1)S(1)} %copy-done.11, bf16[2,4096,128]{2,1,0:T(8,128)(2,1)S(1)} %copy-done.4, f32[2,768,128]{2,1,0:T(8,128)S(1)} %fusion.11), kind=kOutput, calls=%fused_computation.13 | convolution fusion | flops 1611792384 | bytes 15859712 | tf_op jit(solution)/shard_map/erd,edf->erf/dot_general | solution.py:59
  140.6 2.5 convert_element_type.58
  143.1 34.2 %all_to_all.86 = bf16[32,64,512]{2,1,0:T(8,128)(2,1)S(1)} all-to-all(bf16[32,64,512]{2,1,0:T(8,128)(2,1)S(1)} %convert_element_type.58), channel_id=1, replica_groups=mesh['fs'=16,'tp'=8] {'fs'}, dimensions={0} | all-to-all | bytes 4194304 | tf_op jit(solution)/shard_map/all_to_all | solution.py:23
  178.8 3.5 %copy.71 = bf16[2,1024,512]{2,0,1:T(2,128)(2,1)} copy(bf16[2,1024,512]{2,1,0:T(8,128)(2,1)S(1)} %bitcast.51) | data formatting | bytes 4194304 | tf_op jit(solution)/shard_map/all_to_all | solution.py:23
  182.3 5.2 %all-to-all-start.4 = ((bf16[2,1024,512]{2,0,1:T(2,128)(2,1)}), bf16[2,1024,512]{2,0,1:T(2,128)(2,1)S(1)}, u32[]{:S(2)}, u32[]{:S(2)}) async-start(bf16[2,1024,512]{2,0,1:T(2,128)(2,1)} %copy.71), calls=%async_computation.4 | async-start | bytes 4194304 | tf_op jit(solution)/shard_map/all_to_all | solution.py:26
  187.5 4.3 %convolution_convert_fusion.1 = bf16[2,768,512]{2,1,0:T(8,128)(2,1)S(1)} fusion(bf16[2,768,1024]{2,1,0:T(8,128)(2,1)} %all-gather.5.cloned.1.call-done, bf16[2,1024,512]{2,1,0:T(8,128)(2,1)} %bitcast.52), kind=kOutput, calls=%fused_computation.11 | convolution fusion | flops 1611399168 | bytes 6815744 | tf_op jit(solution)/shard_map/erf,efc->erc/dot_general | solution.py:62
  193.1 20.6 %all-to-all-done.4 = bf16[2,1024,512]{2,0,1:T(2,128)(2,1)S(1)} async-done(((bf16[2,1024,512]{2,0,1:T(2,128)(2,1)}), bf16[2,1024,512]{2,0,1:T(2,128)(2,1)S(1)}, u32[]{:S(2)}, u32[]{:S(2)}) %all-to-all-start.4) | async-done | bytes 2097184 | tf_op jit(solution)/shard_map/all_to_all | solution.py:26
  215.0 3.9 %all-to-all-start.3 = ((bf16[512,2,16,48]{0,3,1,2:T(8,128)(2,1)}), bf16[512,2,16,48]{0,3,1,2:T(8,128)(2,1)S(1)}, u32[]{:S(2)}, u32[]{:S(2)}) async-start(bf16[512,2,16,48]{0,3,1,2:T(8,128)(2,1)} %copy.68), calls=%async_computation.3 | async-start | bytes 3145728 | tf_op jit(solution)/shard_map/all_to_all | solution.py:72
  221.0 4.1 %copy.72 = bf16[2,128,8,512]{3,2,1,0:T(8,128)(2,1)} copy(bf16[2,128,8,512]{3,0,1,2:T(2,128)(2,1)} %bitcast.50) | data formatting | bytes 4194304 | tf_op jit(solution)/shard_map/all_to_all | solution.py:26
  225.1 4.2 %all_to_all.78 = bf16[2,128,4096]{2,1,0:T(8,128)(2,1)} reshape(bf16[2,128,8,512]{3,2,1,0:T(8,128)(2,1)} %copy.72) | data formatting | bytes 4194304 | tf_op jit(solution)/shard_map/all_to_all | solution.py:26
  229.3 12.5 %all-to-all-done.3 = bf16[512,2,16,48]{0,3,1,2:T(8,128)(2,1)S(1)} async-done(((bf16[512,2,16,48]{0,3,1,2:T(8,128)(2,1)}), bf16[512,2,16,48]{0,3,1,2:T(8,128)(2,1)S(1)}, u32[]{:S(2)}, u32[]{:S(2)}) %all-to-all-start.3) | async-done | bytes 1572896 | tf_op jit(solution)/shard_map/all_to_all | solution.py:72
  241.8 4.0 %gather_fusion = bf16[1024,512]{1,0:T(8,128)(2,1)S(1)} fusion(bf16[512,1536]{0,1:T(8,128)(2,1)S(1)} %bitcast.47, s32[1024]{0:T(1024)S(1)} %broadcast_clamp_fusion), kind=kCustom, calls=%fused_computation | custom fusion | bytes 2101248 | tf_op jit(solution)/shard_map/jit(_take)/gather | solution.py:74
  246.7 5.2 %multiply_reduce_fusion.1 = bf16[512,512]{1,0:T(8,128)(2,1)} fusion(bf16[512,2,512]{2,1,0:T(2,128)(2,1)S(1)} %reshape.73, pred[512,2]{1,0:T(8,128)(4,1)S(1)} %copy-done.6, f32[512,2]{1,0:T(8,128)S(1)} %copy-done.5), kind=kLoop, calls=%fused_computation.9 | loop fusion | flops 1835008 | bytes 1577984 | tf_op jit(solution)/shard_map/reduce_sum | solution.py:76
  (58 shorter events, 12.3 us)
Async XLA Ops:
  7.2 120.5 %all-gather.3.cloned.1.call-start = ((), (), s32[]{:S(2)}) async-start(), calls=%async_computation.5 | async-start | bytes 14155776 | tf_op jit(solution)/shard_map/all_gather | solution.py:57
  8.4 6.7 %copy-start = (bf16[512,4096]{1,0:T(8,128)(2,1)S(1)}, bf16[512,4096]{1,0:T(8,128)(2,1)}, u32[]{:S(2)}) copy-start(bf16[512,4096]{1,0:T(8,128)(2,1)} %param.8) | copy-start | bytes 12582916
  15.0 10.7 %copy-start.7 = (s32[512,2]{0,1:T(2,128)S(1)}, s32[512,2]{0,1:T(2,128)}, u32[]{:S(2)}) copy-start(s32[512,2]{0,1:T(2,128)} %param.9) | copy-start | bytes 12292
  59.7 1.3 copy-start.10
  61.0 126.5 %all-gather.5.cloned.1.call-start = ((), (), s32[]{:S(2)}) async-start(), calls=%async_computation.6 | async-start | bytes 3538944 | tf_op jit(solution)/shard_map/all_gather | solution.py:64
  121.7 12.5 %copy-start.3 = (bf16[2,4096,128]{2,1,0:T(8,128)(2,1)}, bf16[2,4096,128]{2,1,0:T(8,128)(2,1)S(1)}, u32[]{:S(2)}) copy-start(bf16[2,4096,128]{2,1,0:T(8,128)(2,1)S(1)} %get-tuple-element.6) | copy-start | bytes 6291460
  127.6 6.6 %copy-start.4 = (bf16[2,4096,128]{2,1,0:T(8,128)(2,1)S(1)}, bf16[2,4096,128]{2,1,0:T(8,128)(2,1)}, u32[]{:S(2)}) copy-start(bf16[2,4096,128]{2,1,0:T(8,128)(2,1)} %get-tuple-element.7) | copy-start | bytes 6291460
  127.6 8.8 %copy-start.11 = (bf16[2,768,4096]{2,1,0:T(8,128)(2,1)S(1)}, bf16[2,768,4096]{2,1,0:T(8,128)(2,1)}, u32[]{:S(2)}) copy-start(bf16[2,768,4096]{2,1,0:T(8,128)(2,1)} %all-gather.3.cloned.1.call-done) | copy-start | bytes 37748740
  177.5 1.3 copy-start.2
  182.3 31.4 %all-to-all-start.4 = ((bf16[2,1024,512]{2,0,1:T(2,128)(2,1)}), bf16[2,1024,512]{2,0,1:T(2,128)(2,1)S(1)}, u32[]{:S(2)}, u32[]{:S(2)}) async-start(bf16[2,1024,512]{2,0,1:T(2,128)(2,1)} %copy.71), calls=%async_computation.4 | async-start | bytes 4194304 | tf_op jit(solution)/shard_map/all_to_all | solution.py:26
  193.1 27.0 %copy-start.8 = (f32[512,2]{0,1:T(2,128)S(1)}, f32[512,2]{0,1:T(2,128)}, u32[]{:S(2)}) copy-start(f32[512,2]{0,1:T(2,128)} %param.11) | copy-start | bytes 12292
  193.1 27.0 %copy-start.9 = (f32[512]{0:T(512)S(1)}, f32[512]{0:T(512)}, u32[]{:S(2)}) copy-start(f32[512]{0:T(512)} %param.10) | copy-start | bytes 6148
  213.7 1.3 copy-start.1
  215.0 26.7 %all-to-all-start.3 = ((bf16[512,2,16,48]{0,3,1,2:T(8,128)(2,1)}), bf16[512,2,16,48]{0,3,1,2:T(8,128)(2,1)S(1)}, u32[]{:S(2)}, u32[]{:S(2)}) async-start(bf16[512,2,16,48]{0,3,1,2:T(8,128)(2,1)} %copy.68), calls=%async_computation.3 | async-start | bytes 3145728 | tf_op jit(solution)/shard_map/all_to_all | solution.py:72
  245.7 1.0 copy-start.5
  245.8 0.9 copy-start.6
Sparse Core Ops, SparseCore 0:
  61.1 66.5 all-gather.2
  140.7 31.4 all-gather.4
where the time goes:
time: 260 us; the launch traced here: 259 us
  blocking collectives  117 us (45%)
  waiting for transfers between devices  39 us (15%)
  other arithmetic  31.2 us (12%)
  local copies, waits for them, and re-layouts  30.5 us (12%)
  matrix products  17.3 us (7%)
  between operations  14.3 us (6%)
  starting transfers between devices  9.17 us (4%)
    all_to_all x1, blocking collectives, side_by_side(): lax.all_to_all(both, axis, split_axis=split_dim, concat_axis=concat_dim,...  53.1 us
    all_to_all x1, blocking collectives, on_device(): lax.all_to_all(down_train.astype(jnp.bfloat16), 'fs', split_axis=0, conca...  34.2 us
    all_to_all x1, blocking collectives, on_device(): lax.all_to_all(outgoing.reshape(fs_count, local_experts, capacity, own_co...  30 us
    all_to_all x1, waiting for transfers between devices, on_device(): lax.all_to_all(down_cols, 'tp', split_axis=1, concat_axis=2, tiled=True)  20.6 us
    all_to_all x1, waiting for transfers between devices, on_device(): lax.all_to_all(outgoing_back, 'fs', split_axis=2, concat_axis=1, tiled=True)  12.5 us
    another operation x2, other arithmetic  9.04 us
    all_to_all x2, local copies, waits for them, and re-layouts, on_device(): lax.all_to_all(down_cols, 'tp', split_axis=1, concat_axis=2, tiled=True)  8.26 us
    convert_element_type x1, other arithmetic, on_device(): widened = prompt.astype(jnp.float32)  6.64 us
  transfers between devices with their start and end apart: 4, of which 3 were waited for; matrix products, arithmetic and copies ran while one was open for 10% of the time, Pallas kernels for 0%

commit v1 on v0

v1 whole, which is shorter than its diff:
```python
import jax
import jax.numpy as jnp
from jax import lax
from jax.experimental import pallas as pl
from jax.experimental.pallas import tpu as pltpu
from jax.sharding import PartitionSpec as P

MESH = pl.DeviceIdType.MESH
BF = jnp.bfloat16
F32 = jnp.float32
EPS = 1e-06
CAP = 48
EARLY = (1, 3, 4, 12)
LATE = (2, 5, 6, 7, 8, 9, 10, 11, 13, 14, 15)


def kernel(
    prompt, ids, gw, share, gain, gate, up, down,
    mixed_o, gate_o, up_o, down_o,
    pf, po, xn, gb, sg, su, sd, wsend, dsend, cm, pick, tsend, rows, wrecv, drecv, acc,
    hid, osend, ret, cols, comb, dnew,
    l_p, l_g, l_u, l_d, t_s, t_r, w_s, w_r, x_s, x_r, h_s, h_r, d_s, d_r, n_s, n_r, b_s, b_r, o_s,
):
    f = lax.axis_index("fs")
    t = lax.axis_index("tp")
    z, y = f // 4, f % 4
    x, c = t // 2, t % 2
    right = ((x + 1) % 4) * 2 + c
    left = ((x + 3) % 4) * 2 + c
    across = ((x + 2) % 4) * 2 + c
    mate = x * 2 + 1 - c
    flip = 1 - 2 * c

    def to(k):
        return ((z + k // 4) % 4) * 4 + (y + k % 4) % 4

    def came(k):
        return ((z + 4 - k // 4) % 4) * 4 + (y + 4 - k % 4) % 4

    def at(start, size, unit):
        return pl.ds(pl.multiple_of(start, unit), size)

    def local(src, dst, sem):
        return pltpu.make_async_copy(src, dst, sem)

    def remote(src, dst, ssem, rsem, fs, tp):
        return pltpu.make_async_remote_copy(
            src_ref=src, dst_ref=dst, send_sem=ssem, recv_sem=rsem,
            device_id=(fs, tp), device_id_type=MESH,
        )

    def load_prompt(i):
        return local(prompt.at[pl.ds(i * 128, 128), :], pf.at[pl.ds(i * 128, 128), :], l_p.at[i])

    def load_own():
        return local(prompt.at[:, at(t * 512, 512, 512)], po, l_p.at[4])

    def load_gate(k):
        return local(gate.at[to(k)], sg.at[k], l_g.at[k])

    def load_up(k):
        return local(up.at[to(k)], su.at[k], l_u.at[k])

    def load_down(k, slot):
        return local(down.at[to(k)], sd.at[slot], l_d.at[slot])

    for k in EARLY:
        load_gate(k).start()
        load_up(k).start()
    load_own().start()
    for i in range(4):
        load_prompt(i).start()

    barrier = pltpu.get_barrier_semaphore()

    def greet_fs(k, carry):
        pl.semaphore_signal(barrier, inc=1, device_id=(to(k), t), device_id_type=MESH)
        return carry

    def greet_tp(k, carry):
        pl.semaphore_signal(barrier, inc=1, device_id=(f, (t + k) % 8), device_id_type=MESH)
        return carry

    lax.fori_loop(1, 16, greet_fs, 0)
    lax.fori_loop(1, 8, greet_tp, 0)

    for k in (0,) + LATE:
        load_gate(k).start()
        load_up(k).start()
    for k in range(8):
        load_down(k, k).start()

    gb[...] = jnp.broadcast_to(gain[...], (128, 256)).T

    def cast_weights(k):
        load_gate(k).wait()
        load_up(k).wait()
        for e in range(2):
            wsend[k, e, 0] = (sg[k, e] * gb[...]).astype(BF)
            wsend[k, e, 1] = (su[k, e] * gb[...]).astype(BF)

    def weights_copy(k):
        return remote(
            wsend.at[k], wrecv.at[:, :, at(f * 256, 256, 256), :], w_s.at[k], w_r.at[k], to(k), t
        )

    for k in EARLY:
        cast_weights(k)
    pl.semaphore_wait(barrier, 22)
    for k in EARLY:
        weights_copy(k).start()

    def rank_slots():
        expert = lax.broadcasted_iota(jnp.int32, (32, 512), 0)
        hit0 = ids[0:1, :] == expert
        hit1 = ids[1:2, :] == expert
        named = jnp.where(hit0 | hit1, 1.0, 0.0)
        before = jnp.where(
            lax.broadcasted_iota(jnp.int32, (512, 512), 0)
            < lax.broadcasted_iota(jnp.int32, (512, 512), 1), 1.0, 0.0,
        ).astype(BF)
        count = jnp.dot(named.astype(BF), before, preferred_element_type=F32)
        cm[...] = jnp.where(named > 0.5, count, -1.0)
        total = share[0:1, :] + share[1:2, :]
        for k, hit in ((0, hit0), (1, hit1)):
            rank = jnp.sum(jnp.where(hit, count, 0.0), axis=0, keepdims=True)
            cols[k : k + 1, :] = ids[k : k + 1, :].astype(F32) * float(CAP) + rank
            cols[k + 2 : k + 3, :] = gw[...] * share[k : k + 1, :] / total

    cols[...] = jnp.zeros_like(cols)
    rank_slots()

    def build_pick(e, carry):
        slot = lax.broadcasted_iota(jnp.int32, (CAP, 512), 0).astype(F32)
        pick[e] = jnp.where(cm[pl.ds(e, 1), :] == slot, 1.0, 0.0).astype(BF)
        return carry

    lax.fori_loop(0, 32, build_pick, 0)

    load_own().wait()
    for i in range(4):
        load_prompt(i).wait()

    def normalize(i, carry):
        block = at(i * 32, 32, 32)
        squares = jnp.zeros((32, 128), F32)
        for j in range(32):
            part = pf[block, j * 128 : (j + 1) * 128].astype(F32)
            squares = squares + part * part
        mean = jnp.sum(squares, axis=1, keepdims=True) * (1.0 / 4096.0)
        xn[block, :] = (po[block, :].astype(F32) * lax.rsqrt(mean + EPS)).astype(BF)
        return carry

    lax.fori_loop(0, 16, normalize, 0)

    def token_copy(k):
        return remote(
            tsend.at[k // 4, (y + k % 4) % 4],
            rows.at[t, :, at(f * CAP, CAP, CAP), :],
            t_s.at[k], t_r.at[k], to(k), t,
        )

    for g in range(4):
        chosen = pick[pl.ds(((z + g) % 4) * 8, 8)].reshape(384, 512)
        tsend[g] = (
            jnp.dot(chosen, xn[...], preferred_element_type=F32).astype(BF).reshape(4, 2, CAP, 512)
        )
        for gy in range(4):
            if g + gy:
                token_copy(4 * g + gy).start()
    rows[t, :, at(f * CAP, CAP, CAP), :] = tsend[0, y]

    for k in LATE:
        cast_weights(k)
        weights_copy(k).start()
    cast_weights(0)
    wrecv[:, :, at(f * 256, 256, 256), :] = wsend[0]

    def block_rows(g):
        return at(((z + 4 - g) % 4) * 192, 192, 192)

    def row_copy(g, n):
        r = block_rows(g)
        both = {0: (t, right), 1: (t, left), 2: (t, mate), 3: (left, mate), 5: (right, mate)}
        if n in both:
            s, who = both[n]
            ref = rows.at[s, :, r, :]
        else:
            s, e, who = {4: (left, 0, right), 6: (right, 1, left), 7: (across, 0, mate), 8: (across, 1, mate)}[n]
            ref = rows.at[s, e, r, :]
        return remote(ref, ref, x_s.at[g, n], x_r.at[g, n], f, who)

    def row_arrival(g, n):
        r = block_rows(g)
        both = {0: left, 1: right, 2: mate, 3: left + flip, 5: right + flip}
        if n in both:
            ref = rows.at[both[n], :, r, :]
        else:
            s, e = {4: (across, 0), 6: (across, 1), 7: (across + flip, 0), 8: (across + flip, 1)}[n]
            ref = rows.at[s, e, r, :]
        return remote(ref, ref, x_s.at[g, n], x_r.at[g, n], f, mate)

    def token_arrival(k):
        ref = rows.at[t, :, at(came(k) * CAP, CAP, CAP), :]
        return remote(tsend.at[0, 0], ref, t_s.at[k], t_r.at[k], f, mate)

    for g in range(4):
        for gy in range(4):
            if g + gy:
                token_arrival(4 * g + gy).wait_recv()
        for n in range(3):
            row_copy(g, n).start()

    def down_copy(k):
        return remote(
            dsend.at[k], drecv.at[:, at(f * 64, 64, 64), :], d_s.at[k], d_r.at[k], to(k), t
        )

    def relay(g):
        row_arrival(g, 0).wait_recv()
        row_copy(g, 3).start()
        row_copy(g, 4).start()
        row_arrival(g, 1).wait_recv()
        row_copy(g, 5).start()
        row_copy(g, 6).start()

    def cast_down(k, slot):
        load_down(k, slot).wait()
        for e in range(2):
            dsend[k, e] = sd[slot, e].astype(BF)

    relay(0)
    for k in range(8):
        cast_down(k, k)
    for k in range(8, 16):
        load_down(k, k - 8).start()
    relay(1)
    for k in range(8, 16):
        cast_down(k, k - 8)
    drecv[:, at(f * 64, 64, 64), :] = dsend[0]
    relay(2)
    for k in range(1, 16):
        down_copy(k).start()
    cols_t = cols[...].T
    lane = lax.broadcasted_iota(jnp.int32, (512, 1536), 1).astype(F32)
    for k in range(2):
        comb[k] = jnp.where(cols_t[:, k : k + 1] == lane, 1.0, 0.0).astype(BF)
    relay(3)
    for g in range(4):
        row_arrival(g, 4).wait_recv()
        row_copy(g, 7).start()
        row_arrival(g, 6).wait_recv()
        row_copy(g, 8).start()

    def weights_arrival(k):
        ref = wrecv.at[:, :, at(came(k) * 256, 256, 256), :]
        return remote(wsend.at[k], ref, w_s.at[k], w_r.at[k], f, mate)

    for k in range(1, 16):
        weights_arrival(k).wait_recv()
    gate_out = local(wrecv.at[:, 0], gate_o, o_s.at[0])
    up_out = local(wrecv.at[:, 1], up_o, o_s.at[1])
    gate_out.start()
    up_out.start()
    for g in range(4):
        for n in (2, 3, 5, 7, 8):
            row_arrival(g, n).wait_recv()

    def hidden_copy(n):
        s, e, who = (
            (t, 0, right), (t, 1, right), (t, 1, left), (t, 0, left), (t, 0, mate), (t, 1, mate),
            (left, 0, mate), (left, 0, right), (left, 1, mate), (right, 1, mate), (right, 1, left),
            (right, 0, mate), (across, 0, mate), (across, 1, mate),
        )[n]
        ref = hid.at[s, e]
        return remote(ref, ref, h_s.at[n], h_r.at[n], f, who)

    def hidden_arrival(n):
        s, e = (
            (left, 0), (left, 1), (right, 1), (right, 0), (mate, 0), (mate, 1),
            (left + flip, 0), (across, 0), (left + flip, 1), (right + flip, 1), (across, 1),
            (right + flip, 0), (across + flip, 0), (across + flip, 1),
        )[n]
        ref = hid.at[s, e]
        return remote(ref, ref, h_s.at[n], h_r.at[n], f, mate)

    acc[...] = jnp.zeros_like(acc)
    for e in range(2):

        def project(s, carry):
            part = at(s * 512, 512, 512)
            both = jnp.concatenate([wrecv[e, 0, part, :], wrecv[e, 1, part, :]], axis=1)
            acc[e] += jnp.dot(rows[s, e], both, preferred_element_type=F32)
            return carry

        lax.fori_loop(0, 8, project, 0)
        v = acc[e, :, 0:128]
        hid[t, e] = (v / (1.0 + jnp.exp(-v)) * acc[e, :, 128:256]).astype(BF)

    for n in range(6):
        hidden_copy(n).start()
    for n, onward in ((0, (6, 7)), (2, (9, 10)), (1, (8,)), (3, (11,)), (7, (12,)), (10, (13,))):
        hidden_arrival(n).wait_recv()
        for m in onward:
            hidden_copy(m).start()

    def down_arrival(k):
        ref = drecv.at[:, at(came(k) * 64, 64, 64), :]
        return remote(dsend.at[k], ref, d_s.at[k], d_r.at[k], f, mate)

    for k in range(1, 16):
        down_arrival(k).wait_recv()
    for n in (4, 5, 6, 8, 9, 11, 12, 13):
        hidden_arrival(n).wait_recv()

    def new_copy(k):
        s = (t + k) % 8
        return remote(
            drecv.at[:, at(s * 128, 128, 128), :], dnew.at[t], n_s.at[k], n_r.at[k], f, s
        )

    def back_copy(k):
        return remote(
            osend.at[k // 4, :, at(((y + k % 4) % 4) * CAP, CAP, CAP), :],
            ret.at[pl.ds(2 * f, 2)], b_s.at[k], b_r.at[k], to(k), t,
        )

    for g in range(4):
        part = at(((z + g) % 4) * 192, 192, 192)
        for e in range(2):
            h = jnp.concatenate([hid[s, e, part, :] for s in range(8)], axis=1)
            osend[g, e] = jnp.dot(h, drecv[e], preferred_element_type=F32).astype(BF)
        for gy in range(4):
            if g + gy:
                back_copy(4 * g + gy).start()
    ret[pl.ds(2 * f, 2)] = osend[0, :, at(y * CAP, CAP, CAP), :]
    for k in range(1, 8):
        new_copy(k).start()
    dnew[t] = drecv[:, at(t * 128, 128, 128), :]

    def new_out(s):
        return local(dnew.at[s], down_o.at[:, :, pl.ds(s * 512, 512)], o_s.at[2 + s])

    def new_arrival(k):
        return remote(
            drecv.at[:, pl.ds(0, 128), :], dnew.at[(t + 8 - k) % 8], n_s.at[k], n_r.at[k], f, mate
        )

    def back_arrival(k):
        return remote(
            osend.at[0, :, pl.ds(0, CAP), :], ret.at[pl.ds(2 * came(k), 2)], b_s.at[k], b_r.at[k], f, mate
        )

    for k in range(1, 16):
        back_arrival(k).wait_recv()
    w_t = cols[...].T
    back = ret[...].reshape(1536, 512)
    first = jnp.dot(comb[0], back, preferred_element_type=F32) * w_t[:, 2:3]
    second = jnp.dot(comb[1], back, preferred_element_type=F32) * w_t[:, 3:4]
    mixed_o[...] = (first + second).astype(BF)

    for k in range(1, 8):
        new_arrival(k).wait_recv()
    for s in range(8):
        new_out(s).start()

    for k in range(1, 16):
        token_copy(k).wait_send()
        weights_copy(k).wait_send()
        down_copy(k).wait_send()
        back_copy(k).wait_send()
    for g in range(4):
        for n in range(9):
            row_copy(g, n).wait_send()
    for n in range(14):
        hidden_copy(n).wait_send()
    for k in range(1, 8):
        new_copy(k).wait_send()
    gate_out.wait()
    up_out.wait()
    for s in range(8):
        new_out(s).wait()


def on_device(
    prompt, expert_ids, group_weight, expert_share, norm_gain, gate_train, up_train, down_train
):
    any_ref = pl.BlockSpec(memory_space=pl.ANY)
    vmem_ref = pl.BlockSpec(memory_space=pltpu.VMEM)
    dma = pltpu.SemaphoreType.DMA
    return pl.pallas_call(
        kernel,
        out_shape=(
            jax.ShapeDtypeStruct((512, 512), BF),
            jax.ShapeDtypeStruct((2, 4096, 128), BF),
            jax.ShapeDtypeStruct((2, 4096, 128), BF),
            jax.ShapeDtypeStruct((2, 128, 4096), BF),
        ),
        in_specs=[any_ref, vmem_ref, vmem_ref, vmem_ref, vmem_ref, any_ref, any_ref, any_ref],
        out_specs=(vmem_ref, any_ref, any_ref, any_ref),
        scratch_shapes=[
            pltpu.VMEM((512, 4096), BF),
            pltpu.VMEM((512, 512), BF),
            pltpu.VMEM((512, 512), BF),
            pltpu.VMEM((256, 128), F32),
            pltpu.VMEM((16, 2, 256, 128), F32),
            pltpu.VMEM((16, 2, 256, 128), F32),
            pltpu.VMEM((8, 2, 64, 512), F32),
            pltpu.VMEM((16, 2, 2, 256, 128), BF),
            pltpu.VMEM((16, 2, 64, 512), BF),
            pltpu.VMEM((32, 512), F32),
            pltpu.VMEM((32, CAP, 512), BF),
            pltpu.VMEM((4, 4, 2, CAP, 512), BF),
            pltpu.VMEM((8, 2, 768, 512), BF),
            pltpu.VMEM((2, 2, 4096, 128), BF),
            pltpu.VMEM((2, 1024, 512), BF),
            pltpu.VMEM((2, 768, 256), F32),
            pltpu.VMEM((8, 2, 768, 128), BF),
            pltpu.VMEM((4, 2, 192, 512), BF),
            pltpu.VMEM((32, CAP, 512), BF),
            pltpu.VMEM((128, 512), F32),
            pltpu.VMEM((2, 512, 1536), BF),
            pltpu.VMEM((8, 2, 128, 512), BF),
            dma((5,)), dma((16,)), dma((16,)), dma((8,)),
            dma((16,)), dma((16,)), dma((16,)), dma((16,)),
            dma((4, 9)), dma((4, 9)), dma((14,)), dma((14,)),
            dma((16,)), dma((16,)), dma((8,)), dma((8,)),
            dma((16,)), dma((16,)), dma((10,)),
        ],
        compiler_params=pltpu.CompilerParams(
            collective_id=0, has_side_effects=True, vmem_limit_bytes=67043328
        ),
        name="handover",
    )(
        prompt,
        expert_ids.T,
        group_weight.reshape(1, -1),
        expert_share.T,
        norm_gain.reshape(1, -1),
        gate_train.reshape(16, 2, 256, 128),
        up_train.reshape(16, 2, 256, 128),
        down_train.reshape(16, 2, 64, 512),
    )


def solution(mesh):
    placed = (
        P("fs", None),
        P("fs", None),
        P("fs"),
        P("fs", None),
        P("fs"),
        P(None, "fs", "tp"),
        P(None, "fs", "tp"),
        P(None, "fs", "tp"),
    )
    return jax.shard_map(
        on_device,
        mesh=mesh,
        in_specs=placed,
        out_specs=(P("fs", "tp"), P("fs", None, "tp"), P("fs", None, "tp"), P("fs", "tp", None)),
        check_vma=False,
    )
```

time: 260 us -> 163 us (0.63)
  Pallas kernels: 0 us -> 152 us
  blocking collectives: 117 us -> 0 us
  waiting for transfers between devices: 39 us -> 0 us
  other arithmetic: 31.2 us -> 0 us
  local copies, waits for them, and re-layouts: 30.5 us -> 8.73 us
  matrix products: 17.3 us -> 0 us
  between operations: 14.3 us -> 0.65 us
  starting transfers between devices: 9.17 us -> 0 us
    pallas_call x0 -> x1, Pallas kernels: none -> 152 us  [on_device(): pl.pallas_call(kernel, out_shape=(jax.ShapeDtypeStruct((512, 512), BF), j...]
    all_to_all x3 -> x0, blocking collectives: 117 us -> none  [the longest x1 53.1 us: side_by_side(): lax.all_to_all(both, axis, split_axis=split_dim, concat_axis=concat_dim,...]
    all_to_all x2 -> x0, waiting for transfers between devices: 33.1 us -> none  [the longest x1 20.6 us: on_device(): lax.all_to_all(down_cols, 'tp', split_axis=1, concat_axis=2, tiled=True)]
    dot_general x4 -> x0, matrix products: 17.3 us -> none  [the longest x1 6.55 us: on_device(): jnp.einsum('erd,edf->erf', piece, gate_new, preferred_element_type=jnp.fl...]
    convert_element_type x4 -> x0, other arithmetic: 13.8 us -> none  [the longest x1 6.64 us: on_device(): widened = prompt.astype(jnp.float32)]
    all_to_all x6 -> x0, local copies, waits for them, and re-layouts: 13.6 us -> none  [the longest x2 8.26 us: on_device(): lax.all_to_all(down_cols, 'tp', split_axis=1, concat_axis=2, tiled=True)]
    all_to_all x2 -> x0, starting transfers between devices: 9.09 us -> none  [the longest x1 5.16 us: on_device(): lax.all_to_all(down_cols, 'tp', split_axis=1, concat_axis=2, tiled=True)]
    another operation x2 -> x0, other arithmetic: 9.04 us -> none
  transfers between devices with their start and end apart: 4 -> 0, of which waited for: 3 -> 0; matrix products, arithmetic and copies ran while one was open for 10% -> 0% of each run, Pallas kernels for 0% -> 0%
where the time goes in v1:
time: 163 us; the launch traced here: 161 us
  Pallas kernels  152 us (93%)
  local copies, waits for them, and re-layouts  8.73 us (5%)
    pallas_call x1, Pallas kernels, on_device(): pl.pallas_call(kernel, out_shape=(jax.ShapeDtypeStruct((512, 512), BF), j...  152 us
    unnamed x8, local copies, waits for them, and re-layouts  8.73 us

profile of v1, /device:TPU:1, one launch (start us, length us, event | category | flops | bytes accessed | tf_op | source)
XLA Modules:
  0.0 161.0 jit_solution(2517314944166108427)
XLA Ops:
  0.6 151.6 %handover.1 = (bf16[512,512]{1,0:T(8,128)(2,1)}, bf16[2,4096,128]{2,1,0:T(8,128)(2,1)}, bf16[2,4096,128]{2,1,0:T(8,128)(2,1)}, bf16[2,128,4096]{2,1,0:T(8,128)(2,1)}) custom-call(bf16[512,4096]{1,0:T(8,128)(2,1)} %prompt.1, s32[2,512]{1,0:T(2,128)} %bitcast.10, f32[1,512]{1,0:T(1,128)} %bitcast.12, f32[2,512]{1,0:T(2,128)} %bitcast.11, f32[1,256]{1,0:T(1,128)} %bitcast.13, ...), custom_call_target="tpu_custom_call" | custom-call | tf_op jit(solution)/shard_map/handover/pallas_call | solution.py:391
  152.3 1.9 %copy.16 = bf16[512,512]{1,0:T(8,128)(2,1)} copy(bf16[512,512]{1,0:T(8,128)(2,1)} %get-tuple-element.8) | data formatting | bytes 1048576
  154.1 0.0 copy-start.1
  154.1 3.2 %copy.17 = bf16[2,4096,128]{2,1,0:T(8,128)(2,1)} copy(bf16[2,4096,128]{2,1,0:T(8,128)(2,1)} %get-tuple-element.9) | data formatting | bytes 4194304
  157.3 0.0 copy-done.1
  157.3 0.0 copy-start
  157.3 1.3 copy.18
  158.6 1.0 copy-done
  159.7 1.3 copy.19
Async XLA Ops:
  154.1 3.2 %copy-start.1 = (bf16[2,4096,128]{2,1,0:T(8,128)(2,1)S(1)}, bf16[2,4096,128]{2,1,0:T(8,128)(2,1)}, u32[]{:S(2)}) copy-start(bf16[2,4096,128]{2,1,0:T(8,128)(2,1)} %get-tuple-element.10) | copy-start | bytes 6291460
  157.3 2.3 %copy-start = (bf16[2,128,4096]{2,1,0:T(8,128)(2,1)S(1)}, bf16[2,128,4096]{2,1,0:T(8,128)(2,1)}, u32[]{:S(2)}) copy-start(bf16[2,128,4096]{2,1,0:T(8,128)(2,1)} %get-tuple-element.11) | copy-start | bytes 6291460

commit v2 on v1

v2 whole, which is shorter than its diff:
```python
import jax
import jax.numpy as jnp
from jax import lax
from jax.experimental import pallas as pl
from jax.experimental.pallas import tpu as pltpu
from jax.sharding import PartitionSpec as P

MESH = pl.DeviceIdType.MESH
BF = jnp.bfloat16
F32 = jnp.float32
EPS = 1e-06
CAP = 48
ORDER = (4, 12, 1, 3, 5, 15, 7, 13, 8, 2, 10, 6, 14, 9, 11)


def kernel(
    prompt, ids, gw, share, gain, gate, up, down,
    mixed_o, gate_o, up_o, down_o,
    pf, po, xn, gb, sg, su, sd, wsend, dsend, cm, pick, tsend, rows, wrecv, drecv, acc,
    hid, osend, ret, cols, comb, macc, dnew,
    l_p, l_g, l_u, l_d, t_s, t_r, w_s, w_r, x_s, x_r, h_s, h_r, d_s, d_r, n_s, n_r, b_s, b_r, o_s,
):
    f = lax.axis_index("fs")
    t = lax.axis_index("tp")
    z, y = f // 4, f % 4
    x, c = t // 2, t % 2
    right = ((x + 1) % 4) * 2 + c
    left = ((x + 3) % 4) * 2 + c
    across = ((x + 2) % 4) * 2 + c
    mate = x * 2 + 1 - c
    flip = 1 - 2 * c

    def to(k):
        return ((z + k // 4) % 4) * 4 + (y + k % 4) % 4

    def came(k):
        return ((z + 4 - k // 4) % 4) * 4 + (y + 4 - k % 4) % 4

    def at(start, size, unit):
        return pl.ds(pl.multiple_of(start, unit), size)

    def local(src, dst, sem):
        return pltpu.make_async_copy(src, dst, sem)

    def remote(src, dst, ssem, rsem, fs, tp):
        return pltpu.make_async_remote_copy(
            src_ref=src, dst_ref=dst, send_sem=ssem, recv_sem=rsem,
            device_id=(fs, tp), device_id_type=MESH,
        )

    def load_prompt(i):
        return local(prompt.at[pl.ds(i * 128, 128), :], pf.at[pl.ds(i * 128, 128), :], l_p.at[i])

    def load_own():
        return local(prompt.at[:, at(t * 512, 512, 512)], po, l_p.at[4])

    def load_gate(k):
        return local(gate.at[to(k)], sg.at[k], l_g.at[k])

    def load_up(k):
        return local(up.at[to(k)], su.at[k], l_u.at[k])

    def load_down(k, slot):
        return local(down.at[to(k)], sd.at[slot], l_d.at[slot])

    load_own().start()
    for i in range(4):
        load_prompt(i).start()

    barrier = pltpu.get_barrier_semaphore()

    def greet_fs(k, carry):
        pl.semaphore_signal(barrier, inc=1, device_id=(to(k), t), device_id_type=MESH)
        return carry

    def greet_tp(k, carry):
        pl.semaphore_signal(barrier, inc=1, device_id=(f, (t + k) % 8), device_id_type=MESH)
        return carry

    lax.fori_loop(1, 16, greet_fs, 0)
    lax.fori_loop(1, 8, greet_tp, 0)

    for k in ORDER + (0,):
        load_gate(k).start()
        load_up(k).start()
    for k in range(8):
        load_down(k, k).start()

    gb[...] = jnp.broadcast_to(gain[...], (128, 256)).T

    def rank_slots():
        expert = lax.broadcasted_iota(jnp.int32, (32, 512), 0)
        hit0 = ids[0:1, :] == expert
        hit1 = ids[1:2, :] == expert
        named = jnp.where(hit0 | hit1, 1.0, 0.0)
        before = jnp.where(
            lax.broadcasted_iota(jnp.int32, (512, 512), 0)
            < lax.broadcasted_iota(jnp.int32, (512, 512), 1), 1.0, 0.0,
        ).astype(BF)
        count = jnp.dot(named.astype(BF), before, preferred_element_type=F32)
        cm[...] = jnp.where(named > 0.5, count, -1.0)
        total = share[0:1, :] + share[1:2, :]
        for k, hit in ((0, hit0), (1, hit1)):
            rank = jnp.sum(jnp.where(hit, count, 0.0), axis=0, keepdims=True)
            expert_of = ids[k : k + 1, :]
            place = (expert_of & 1) * 768 + (expert_of >> 1) * CAP
            cols[k : k + 1, :] = place.astype(F32) + rank
            cols[k + 2 : k + 3, :] = gw[...] * share[k : k + 1, :] / total

    cols[...] = jnp.zeros_like(cols)
    rank_slots()

    def build_pick(e, carry):
        slot = lax.broadcasted_iota(jnp.int32, (CAP, 512), 0).astype(F32)
        pick[e] = jnp.where(cm[pl.ds(e, 1), :] == slot, 1.0, 0.0).astype(BF)
        return carry

    lax.fori_loop(0, 32, build_pick, 0)

    load_own().wait()
    for i in range(4):
        load_prompt(i).wait()

    def normalize(i, carry):
        block = at(i * 32, 32, 32)
        squares = jnp.zeros((32, 128), F32)
        for j in range(32):
            part = pf[block, j * 128 : (j + 1) * 128].astype(F32)
            squares = squares + part * part
        mean = jnp.sum(squares, axis=1, keepdims=True) * (1.0 / 4096.0)
        xn[block, :] = (po[block, :].astype(F32) * lax.rsqrt(mean + EPS)).astype(BF)
        return carry

    lax.fori_loop(0, 16, normalize, 0, unroll=4)

    for g in range(4):
        chosen = pick[g * 8 : g * 8 + 8].reshape(384, 512)
        tsend[4 * g : 4 * g + 4] = (
            jnp.dot(chosen, xn[...], preferred_element_type=F32).astype(BF).reshape(4, 2, CAP, 512)
        )

    def token_copy(k):
        return remote(
            tsend.at[to(k)], rows.at[t, :, at(f * CAP, CAP, CAP), :],
            t_s.at[k], t_r.at[k], to(k), t,
        )

    pl.semaphore_wait(barrier, 22)
    for k in ORDER:
        token_copy(k).start()
    rows[t, :, at(f * CAP, CAP, CAP), :] = tsend[f]

    def cast_weights(k, e):
        wsend[k, e, 0] = (sg[k, e] * gb[...]).astype(BF)
        wsend[k, e, 1] = (su[k, e] * gb[...]).astype(BF)

    def weights_copy(k, e, m):
        return remote(
            wsend.at[k, e, m], wrecv.at[e, m, at(f * 256, 256, 256), :],
            w_s.at[e, k], w_r.at[e, k], to(k), t,
        )

    def weights_pair(k, e):
        return remote(
            wsend.at[k, e], wrecv.at[e, :, at(came(k) * 256, 256, 256), :],
            w_s.at[e, k], w_r.at[e, k], to(k), t,
        )

    for k in ORDER + (0,):
        load_gate(k).wait()
        load_up(k).wait()
        cast_weights(k, 0)
    for m in range(2):
        for k in ORDER:
            weights_copy(k, 0, m).start()
    for k in ORDER + (0,):
        cast_weights(k, 1)
    wrecv[:, :, at(f * 256, 256, 256), :] = wsend[0]
    for m in range(2):
        for k in ORDER:
            weights_copy(k, 1, m).start()

    def row_copy(k, n):
        r = at(came(k) * CAP, CAP, CAP)
        both = {0: (t, right), 1: (t, left), 2: (t, mate), 3: (left, mate), 5: (right, mate)}
        if n in both:
            s, who = both[n]
            ref = rows.at[s, :, r, :]
        else:
            s, e, who = {4: (left, 0, right), 6: (right, 1, left), 7: (across, 0, mate), 8: (across, 1, mate)}[n]
            ref = rows.at[s, e, r, :]
        return remote(ref, ref, x_s.at[k, n], x_r.at[k, n], f, who)

    def row_arrival(k, n):
        r = at(came(k) * CAP, CAP, CAP)
        both = {0: left, 1: right, 2: mate, 3: left + flip, 5: right + flip}
        if n in both:
            ref = rows.at[both[n], :, r, :]
        else:
            s, e = {4: (across, 0), 6: (across, 1), 7: (across + flip, 0), 8: (across + flip, 1)}[n]
            ref = rows.at[s, e, r, :]
        return remote(ref, ref, x_s.at[k, n], x_r.at[k, n], f, mate)

    def token_arrival(k):
        ref = rows.at[t, :, at(came(k) * CAP, CAP, CAP), :]
        return remote(tsend.at[0], ref, t_s.at[k], t_r.at[k], f, mate)

    for k in (0,) + ORDER:
        if k:
            token_arrival(k).wait_recv()
        for n in range(3):
            row_copy(k, n).start()

    def down_copy(k, e):
        return remote(
            dsend.at[k, e], drecv.at[e, at(f * 64, 64, 64), :], d_s.at[e, k], d_r.at[e, k], to(k), t
        )

    def cast_down(k, slot):
        load_down(k, slot).wait()
        for e in range(2):
            dsend[k, e] = sd[slot, e].astype(BF)

    def relay(k):
        row_arrival(k, 0).wait_recv()
        row_copy(k, 4).start()
        row_copy(k, 3).start()
        row_arrival(k, 1).wait_recv()
        row_copy(k, 6).start()
        row_copy(k, 5).start()

    for k in range(8):
        cast_down(k, k)
    for k in range(8, 16):
        load_down(k, k - 8).start()
    chain = (0,) + ORDER
    for k in chain[:6]:
        relay(k)
    for k in range(8, 16):
        cast_down(k, k - 8)
    drecv[:, at(f * 64, 64, 64), :] = dsend[0]
    for e in range(2):
        for k in ORDER:
            down_copy(k, e).start()
    for k in chain[6:11]:
        relay(k)
    cols_t = cols[...].T
    lane = lax.broadcasted_iota(jnp.int32, (512, 768), 1).astype(F32)
    for k in range(2):
        for e in range(2):
            comb[k, e] = jnp.where(cols_t[:, k : k + 1] == lane + 768.0 * e, 1.0, 0.0).astype(BF)
    for k in chain[11:]:
        relay(k)

    def project(e, chip):
        part = at(chip * 1024, 1024, 1024)
        left_side = jnp.concatenate([rows[2 * chip, e], rows[2 * chip + 1, e]], axis=1)
        both = jnp.concatenate([wrecv[e, 0, part, :], wrecv[e, 1, part, :]], axis=1)
        return jnp.dot(left_side, both, preferred_element_type=F32)

    def near(e):
        acc[e] = project(e, x)

        def step(j, carry):
            acc[e] += project(e, (x + j + j // 2) % 4)
            return carry

        lax.fori_loop(1, 3, step, 0)

    def finish(e):
        acc[e] += project(e, (x + 2) % 4)
        v = acc[e, :, 0:128]
        hid[t, e] = (v / (1.0 + jnp.exp(-v)) * acc[e, :, 128:256]).astype(BF)

    def hidden_ref(s, e, part):
        return hid.at[s, e] if part is None else hid.at[s, e, pl.ds(part * 384, 384), :]

    def hidden_copy(e, n):
        s, part, who = (
            (t, None, right), (t, None, left), (t, None, mate), (left, None, mate), (left, 0, right),
            (right, None, mate), (right, 1, left), (across, 0, mate), (across, 1, mate),
        )[n]
        ref = hidden_ref(s, e, part)
        return remote(ref, ref, h_s.at[e, n], h_r.at[e, n], f, who)

    def hidden_arrival(e, n):
        s, part = (
            (left, None), (right, None), (mate, None), (left + flip, None), (across, 0),
            (right + flip, None), (across, 1), (across + flip, 0), (across + flip, 1),
        )[n]
        ref = hidden_ref(s, e, part)
        return remote(ref, ref, h_s.at[e, n], h_r.at[e, n], f, mate)

    for k in ORDER:
        weights_pair(k, 0).wait_recv()
    for k in chain:
        for n in (2, 3, 5):
            row_arrival(k, n).wait_recv()
    near(0)
    for k in chain:
        row_arrival(k, 4).wait_recv()
        row_copy(k, 7).start()
        row_arrival(k, 6).wait_recv()
        row_copy(k, 8).start()
    for k in chain:
        for n in (7, 8):
            row_arrival(k, n).wait_recv()
    finish(0)
    for n in range(3):
        hidden_copy(0, n).start()
    for k in ORDER:
        weights_pair(k, 1).wait_recv()
    gate_out = local(wrecv.at[:, 0], gate_o, o_s.at[0])
    up_out = local(wrecv.at[:, 1], up_o, o_s.at[1])
    near(1)
    finish(1)
    for n in range(3):
        hidden_copy(1, n).start()
    gate_out.start()
    up_out.start()

    for e in range(2):
        hidden_arrival(e, 0).wait_recv()
        hidden_copy(e, 4).start()
        hidden_copy(e, 3).start()
        hidden_arrival(e, 1).wait_recv()
        hidden_copy(e, 6).start()
        hidden_copy(e, 5).start()

    def down_arrival(k, e):
        ref = drecv.at[e, at(came(k) * 64, 64, 64), :]
        return remote(dsend.at[k, e], ref, d_s.at[e, k], d_r.at[e, k], f, mate)

    def new_copy(k, e):
        s = (t + k) % 8
        return remote(
            drecv.at[e, at(s * 128, 128, 128), :], dnew.at[t, e], n_s.at[e, k], n_r.at[e, k], f, s
        )

    def new_arrival(k, e):
        return remote(
            drecv.at[e, pl.ds(0, 128), :], dnew.at[(t + 8 - k) % 8, e],
            n_s.at[e, k], n_r.at[e, k], f, mate,
        )

    def back_copy(k, e):
        return remote(
            osend.at[e, at(to(k) * CAP, CAP, CAP), :], ret.at[e, f], b_s.at[e, k], b_r.at[e, k], to(k), t
        )

    def back_arrival(k, e):
        return remote(
            osend.at[e, pl.ds(0, CAP), :], ret.at[e, came(k)], b_s.at[e, k], b_r.at[e, k], f, mate
        )

    for e in range(2):
        for n, m in ((4, 7), (6, 8)):
            hidden_arrival(e, n).wait_recv()
            hidden_copy(e, m).start()
        for k in ORDER:
            down_arrival(k, e).wait_recv()
        for n in (2, 3, 5, 7, 8):
            hidden_arrival(e, n).wait_recv()

        def expert_out(g, carry):
            part = at(g * 192, 192, 192)
            h = jnp.concatenate([hid[s, e, part, :] for s in range(8)], axis=1)
            osend[e, part, :] = jnp.dot(h, drecv[e], preferred_element_type=F32).astype(BF)
            return carry

        lax.fori_loop(0, 4, expert_out, 0)
        for k in ORDER:
            back_copy(k, e).start()
        ret[e, f] = osend[e, at(f * CAP, CAP, CAP), :]
        for k in range(1, 8):
            new_copy(k, e).start()
        dnew[t, e] = drecv[e, at(t * 128, 128, 128), :]

    def new_out(s):
        return local(dnew.at[s], down_o.at[:, :, pl.ds(s * 512, 512)], o_s.at[2 + s])

    def mix(e):
        back = ret[e].reshape(768, 512)
        w_t = cols[...].T
        first = jnp.dot(comb[0, e], back, preferred_element_type=F32) * w_t[:, 2:3]
        second = jnp.dot(comb[1, e], back, preferred_element_type=F32) * w_t[:, 3:4]
        return first + second

    for k in ORDER:
        back_arrival(k, 0).wait_recv()
    macc[...] = mix(0)
    for e in range(2):
        for k in range(1, 8):
            new_arrival(k, e).wait_recv()
    for s in range(8):
        new_out(s).start()
    for k in ORDER:
        back_arrival(k, 1).wait_recv()
    mixed_o[...] = (macc[...] + mix(1)).astype(BF)

    for k in ORDER:
        token_copy(k).wait_send()
        for e in range(2):
            weights_pair(k, e).wait_send()
            down_copy(k, e).wait_send()
            back_copy(k, e).wait_send()
    for k in chain:
        for n in range(9):
            row_copy(k, n).wait_send()
    for e in range(2):
        for n in range(9):
            hidden_copy(e, n).wait_send()
        for k in range(1, 8):
            new_copy(k, e).wait_send()
    gate_out.wait()
    up_out.wait()
    for s in range(8):
        new_out(s).wait()


def on_device(
    prompt, expert_ids, group_weight, expert_share, norm_gain, gate_train, up_train, down_train
):
    any_ref = pl.BlockSpec(memory_space=pl.ANY)
    vmem_ref = pl.BlockSpec(memory_space=pltpu.VMEM)
    dma = pltpu.SemaphoreType.DMA
    return pl.pallas_call(
        kernel,
        out_shape=(
            jax.ShapeDtypeStruct((512, 512), BF),
            jax.ShapeDtypeStruct((2, 4096, 128), BF),
            jax.ShapeDtypeStruct((2, 4096, 128), BF),
            jax.ShapeDtypeStruct((2, 128, 4096), BF),
        ),
        in_specs=[any_ref, vmem_ref, vmem_ref, vmem_ref, vmem_ref, any_ref, any_ref, any_ref],
        out_specs=(vmem_ref, any_ref, any_ref, any_ref),
        scratch_shapes=[
            pltpu.VMEM((512, 4096), BF),
            pltpu.VMEM((512, 512), BF),
            pltpu.VMEM((512, 512), BF),
            pltpu.VMEM((256, 128), F32),
            pltpu.VMEM((16, 2, 256, 128), F32),
            pltpu.VMEM((16, 2, 256, 128), F32),
            pltpu.VMEM((8, 2, 64, 512), F32),
            pltpu.VMEM((16, 2, 2, 256, 128), BF),
            pltpu.VMEM((16, 2, 64, 512), BF),
            pltpu.VMEM((32, 512), F32),
            pltpu.VMEM((32, CAP, 512), BF),
            pltpu.VMEM((16, 2, CAP, 512), BF),
            pltpu.VMEM((8, 2, 768, 512), BF),
            pltpu.VMEM((2, 2, 4096, 128), BF),
            pltpu.VMEM((2, 1024, 512), BF),
            pltpu.VMEM((2, 768, 256), F32),
            pltpu.VMEM((8, 2, 768, 128), BF),
            pltpu.VMEM((2, 768, 512), BF),
            pltpu.VMEM((2, 16, CAP, 512), BF),
            pltpu.VMEM((128, 512), F32),
            pltpu.VMEM((2, 2, 512, 768), BF),
            pltpu.VMEM((512, 512), F32),
            pltpu.VMEM((8, 2, 128, 512), BF),
            dma((5,)), dma((16,)), dma((16,)), dma((8,)),
            dma((16,)), dma((16,)), dma((2, 16)), dma((2, 16)),
            dma((16, 9)), dma((16, 9)), dma((2, 9)), dma((2, 9)),
            dma((2, 16)), dma((2, 16)), dma((2, 8)), dma((2, 8)),
            dma((2, 16)), dma((2, 16)), dma((10,)),
        ],
        compiler_params=pltpu.CompilerParams(
            collective_id=0, has_side_effects=True, vmem_limit_bytes=67043328
        ),
        name="handover",
    )(
        prompt,
        expert_ids.T,
        group_weight.reshape(1, -1),
        expert_share.T,
        norm_gain.reshape(1, -1),
        gate_train.reshape(16, 2, 256, 128),
        up_train.reshape(16, 2, 256, 128),
        down_train.reshape(16, 2, 64, 512),
    )


def solution(mesh):
    placed = (
        P("fs", None),
        P("fs", None),
        P("fs"),
        P("fs", None),
        P("fs"),
        P(None, "fs", "tp"),
        P(None, "fs", "tp"),
        P(None, "fs", "tp"),
    )
    return jax.shard_map(
        on_device,
        mesh=mesh,
        in_specs=placed,
        out_specs=(P("fs", "tp"), P("fs", None, "tp"), P("fs", None, "tp"), P("fs", "tp", None)),
        check_vma=False,
    )
```

time: 163 us -> 132 us (0.81); the launches traced: 161 us -> 132 us
  Pallas kernels: 152 us -> 123 us
    pallas_call x1, Pallas kernels: 152 us -> 123 us  [on_device(): pl.pallas_call(kernel, out_shape=(jax.ShapeDtypeStruct((512, 512), BF), j...]
where the time goes in v2:
time: 132 us
  Pallas kernels  123 us (93%)
  local copies, waits for them, and re-layouts  8.73 us (7%)
    pallas_call x1, Pallas kernels, on_device(): pl.pallas_call(kernel, out_shape=(jax.ShapeDtypeStruct((512, 512), BF), j...  123 us
    unnamed x8, local copies, waits for them, and re-layouts  8.73 us

profile of v2, /device:TPU:1, one launch (start us, length us, event | category | flops | bytes accessed | tf_op | source)
XLA Modules:
  0.0 132.1 jit_solution(10779164244424709897)
XLA Ops:
  0.6 122.8 %handover.1 = (bf16[512,512]{1,0:T(8,128)(2,1)}, bf16[2,4096,128]{2,1,0:T(8,128)(2,1)}, bf16[2,4096,128]{2,1,0:T(8,128)(2,1)}, bf16[2,128,4096]{2,1,0:T(8,128)(2,1)}) custom-call(bf16[512,4096]{1,0:T(8,128)(2,1)} %prompt.1, s32[2,512]{1,0:T(2,128)} %bitcast.10, f32[1,512]{1,0:T(1,128)} %bitcast.12, f32[2,512]{1,0:T(2,128)} %bitcast.11, f32[1,256]{1,0:T(1,128)} %bitcast.13, ...), custom_call_target="tpu_custom_call" | custom-call | tf_op jit(solution)/shard_map/handover/pallas_call | solution.py:427
  123.4 1.9 %copy.16 = bf16[512,512]{1,0:T(8,128)(2,1)} copy(bf16[512,512]{1,0:T(8,128)(2,1)} %get-tuple-element.8) | data formatting | bytes 1048576
  125.3 0.0 copy-start.1
  125.3 3.2 %copy.17 = bf16[2,4096,128]{2,1,0:T(8,128)(2,1)} copy(bf16[2,4096,128]{2,1,0:T(8,128)(2,1)} %get-tuple-element.9) | data formatting | bytes 4194304
  128.5 0.0 copy-done.1
  128.5 0.0 copy-start
  128.5 1.3 copy.18
  129.8 1.0 copy-done
  130.8 1.3 copy.19
Async XLA Ops:
  125.3 3.2 %copy-start.1 = (bf16[2,4096,128]{2,1,0:T(8,128)(2,1)S(1)}, bf16[2,4096,128]{2,1,0:T(8,128)(2,1)}, u32[]{:S(2)}) copy-start(bf16[2,4096,128]{2,1,0:T(8,128)(2,1)} %get-tuple-element.10) | copy-start | bytes 6291460
  128.5 2.3 %copy-start = (bf16[2,128,4096]{2,1,0:T(8,128)(2,1)S(1)}, bf16[2,128,4096]{2,1,0:T(8,128)(2,1)}, u32[]{:S(2)}) copy-start(bf16[2,128,4096]{2,1,0:T(8,128)(2,1)} %get-tuple-element.11) | copy-start | bytes 6291460

commit v3 on v2

v3 whole, which is shorter than its diff:
```python
import jax
import jax.numpy as jnp
from jax import lax
from jax.experimental import pallas as pl
from jax.experimental.pallas import tpu as pltpu
from jax.sharding import PartitionSpec as P

MESH = pl.DeviceIdType.MESH
BF = jnp.bfloat16
F32 = jnp.float32
EPS = 1e-06
CAP = 48
ORDER = (4, 12, 1, 3, 5, 15, 7, 13, 8, 2, 10, 6, 14, 9, 11)


def kernel(
    prompt, ids_h, gw_h, share_h, gain_h, gate, up, down,
    gate_o, up_o, down_o, ret1, comb1, macc, shares,
    ids, gw, share, gain, pf, xn, gb, sw, sd, wsend, dsend, cm, tsend, rows, drecv,
    hid, stage, ret0, cols,
    i_s, l_s, s_s, t_r, w_r, x_r, x_b, h_r, d_r, n_r, b_r,
):
    f = lax.axis_index("fs")
    t = lax.axis_index("tp")
    z, y = f // 4, f % 4
    x, c = t // 2, t % 2
    right = ((x + 1) % 4) * 2 + c
    left = ((x + 3) % 4) * 2 + c
    across = ((x + 2) % 4) * 2 + c
    mate = x * 2 + 1 - c
    flip = 1 - 2 * c

    def to(k):
        return ((z + k // 4) % 4) * 4 + (y + k % 4) % 4

    def came(k):
        return ((z + 4 - k // 4) % 4) * 4 + (y + 4 - k % 4) % 4

    def at(start, size, unit):
        return pl.ds(pl.multiple_of(start, unit), size)

    def local(src, dst, sem):
        return pltpu.make_async_copy(src, dst, sem)

    def remote(src, dst, ssem, rsem, fs, tp):
        return pltpu.make_async_remote_copy(
            src_ref=src, dst_ref=dst, send_sem=ssem, recv_sem=rsem,
            device_id=(fs, tp), device_id_type=MESH,
        )

    def arrived(ref, sem):
        remote(ref, ref, s_s.at[0], sem, f, mate).wait_recv()

    def sent(ref, sem):
        remote(ref, ref, sem, n_r.at[0], f, mate).wait_send()

    barrier = pltpu.get_barrier_semaphore()

    def greet_fs(k, carry):
        pl.semaphore_signal(barrier, inc=1, device_id=(to(k), t), device_id_type=MESH)
        return carry

    def greet_tp(k, carry):
        pl.semaphore_signal(barrier, inc=1, device_id=(f, (t + k) % 8), device_id_type=MESH)
        return carry

    lax.fori_loop(1, 16, greet_fs, 0)
    lax.fori_loop(1, 8, greet_tp, 0)

    chain = (0,) + ORDER
    source = (gate, up)
    fresh = (gate_o, up_o)
    ret = (ret0, ret1)
    comb = (pf, comb1)

    def load_weights(i, e, m, sem):
        return local(source[m].at[to(chain[(i + 1) % 16]), e], sw.at[i, m], l_s.at[sem])

    small = [
        local(src, dst, i_s.at[n])
        for n, (src, dst) in enumerate(((ids_h, ids), (gw_h, gw), (share_h, share), (gain_h, gain)))
    ]
    for load in small:
        load.start()
    for i in range(8):
        load_weights(i, 0, 0, 0).start()
    for i in range(16):
        local(prompt.at[:, i * 256 : (i + 1) * 256], pf.at[i], l_s.at[1]).start()
    for i in range(16):
        for m in range(2):
            if i > 7 or m:
                load_weights(i, 0, m, 2).start()

    for load in small:
        load.wait()
    gb[...] = jnp.broadcast_to(gain[...], (128, 256)).T

    def rank_slots():
        expert = lax.broadcasted_iota(jnp.int32, (32, 512), 0)
        hit0 = ids[0:1, :] == expert
        hit1 = ids[1:2, :] == expert
        named = jnp.where(hit0 | hit1, 1.0, 0.0)
        before = jnp.where(
            lax.broadcasted_iota(jnp.int32, (512, 512), 0)
            < lax.broadcasted_iota(jnp.int32, (512, 512), 1), 1.0, 0.0,
        ).astype(BF)
        count = jnp.dot(named.astype(BF), before, preferred_element_type=F32)
        cm[...] = jnp.where(named > 0.5, count, -1.0)
        total = share[0:1, :] + share[1:2, :]
        for k, hit in ((0, hit0), (1, hit1)):
            rank = jnp.sum(jnp.where(hit, count, 0.0), axis=0, keepdims=True)
            expert_of = ids[k : k + 1, :]
            place = (expert_of & 1) * 768 + (expert_of >> 1) * CAP
            cols[k : k + 1, :] = place.astype(F32) + rank
            cols[k + 2 : k + 3, :] = gw[...] * share[k : k + 1, :] / total

    cols[...] = jnp.zeros_like(cols)
    rank_slots()

    def build_pick(e, carry):
        slot = lax.broadcasted_iota(jnp.int32, (CAP, 512), 0).astype(F32)
        stage[e] = jnp.where(cm[pl.ds(e, 1), :] == slot, 1.0, 0.0).astype(BF)
        return carry

    lax.fori_loop(0, 32, build_pick, 0)

    def cast_weights(i, e, m):
        wsend[chain[(i + 1) % 16], e, m] = (sw[i, m] * gb[...]).astype(BF)

    def weights_copy(k, e, m):
        return remote(
            wsend.at[k, e, m], fresh[m].at[e, at(f * 256, 256, 256), :],
            s_s.at[0], w_r.at[e, m], to(k), t,
        )

    local(sw.at[pl.ds(0, 8), 0], sw.at[pl.ds(0, 8), 0], l_s.at[0]).wait()
    for i in range(8):
        cast_weights(i, 0, 0)
    pl.semaphore_wait(barrier, 22)
    for k in ORDER[:8]:
        weights_copy(k, 0, 0).start()

    local(pf, pf, l_s.at[1]).wait()

    def normalize(i, carry):
        block = at(i * 32, 32, 32)
        squares = jnp.zeros((32, 256), F32)
        for j in range(16):
            part = pf[j, block, :].astype(F32)
            squares = squares + part * part
        mean = jnp.sum(squares, axis=1, keepdims=True) * (1.0 / 4096.0)
        scale = lax.rsqrt(mean + EPS)
        for h in range(2):
            part = pf[2 * t + h, block, :].astype(F32)
            xn[block, h * 256 : (h + 1) * 256] = (part * scale).astype(BF)
        return carry

    lax.fori_loop(0, 16, normalize, 0, unroll=4)

    for g in range(4):
        chosen = stage[g * 8 : g * 8 + 8].reshape(384, 512)
        tsend[4 * g : 4 * g + 4] = (
            jnp.dot(chosen, xn[...], preferred_element_type=F32).astype(BF).reshape(4, 2, CAP, 512)
        )

    def token_copy(k):
        return remote(
            tsend.at[to(k)], rows.at[t, :, at(f * CAP, CAP, CAP), :],
            s_s.at[1], t_r.at[k], to(k), t,
        )

    for k in ORDER:
        token_copy(k).start()
    rows[t, :, at(f * CAP, CAP, CAP), :] = tsend[f]

    local(sw.at[pl.ds(0, 12)], sw.at[pl.ds(0, 12)], l_s.at[2]).wait()
    for m in range(2):
        for i in range(16):
            if i > 7 or m:
                cast_weights(i, 0, m)
    for k in ORDER[8:]:
        weights_copy(k, 0, 0).start()
    for k in ORDER:
        weights_copy(k, 0, 1).start()
    for i in range(16):
        for m in range(2):
            load_weights(i, 1, m, 3).start()

    def load_down(i):
        return local(down.at[to(chain[i])], sd.at[pl.ds(i % 8 * 2, 2)], l_s.at[4])

    for i in range(8):
        load_down(i).start()

    def row_copy(k, n):
        r = at(came(k) * CAP, CAP, CAP)
        both = {0: (t, right), 1: (t, left), 2: (t, mate), 3: (left, mate), 5: (right, mate)}
        if n in both:
            s, who = both[n]
            ref = rows.at[s, :, r, :]
        else:
            s, e, who = {4: (left, 0, right), 6: (right, 1, left), 7: (across, 0, mate), 8: (across, 1, mate)}[n]
            ref = rows.at[s, e, r, :]
        slot = {0: 0, 1: 1, 4: 2, 6: 3}
        i = chain.index(k) // 2
        sem = x_r.at[i, slot[n]] if n in slot else x_b.at[n // 7]
        return remote(ref, ref, s_s.at[2], sem, f, who)

    pair = pl.ds(0, 2 * CAP)

    def token_round(part):
        for k in part:
            if k:
                arrived(tsend.at[0], t_r.at[k])
            for n in range(3):
                row_copy(k, n).start()

    token_round(chain[:6])
    local(sw, sw, l_s.at[3]).wait()
    for m in range(2):
        for i in range(16):
            cast_weights(i, 1, m)
        for k in ORDER:
            weights_copy(k, 1, m).start()
    for m in range(2):
        fresh[m][:, at(f * 256, 256, 256), :] = wsend[0, :, m]
    token_round(chain[6:])

    def down_copy(k, e):
        return remote(
            dsend.at[k, e], drecv.at[e, at(f * 64, 64, 64), :], s_s.at[3], d_r.at[e], to(k), t
        )

    def cast_down(base):
        local(sd, sd, l_s.at[4]).wait()
        for i in range(8):
            for e in range(2):
                dsend[chain[base + i], e] = sd[2 * i + e].astype(BF)

    def relay(i):
        arrived(rows.at[left, :, pair, :], x_r.at[i, 0])
        for k in chain[2 * i : 2 * i + 2]:
            row_copy(k, 4).start()
            row_copy(k, 3).start()
        arrived(rows.at[right, :, pair, :], x_r.at[i, 1])
        for k in chain[2 * i : 2 * i + 2]:
            row_copy(k, 6).start()
            row_copy(k, 5).start()

    cast_down(0)
    for i in range(8, 16):
        load_down(i).start()
    for i in range(3):
        relay(i)
    cast_down(8)
    drecv[:, at(f * 64, 64, 64), :] = dsend[0]
    for e in range(2):
        for k in ORDER:
            down_copy(k, e).start()
    for i in range(3, 6):
        relay(i)
    cols_t = cols[...].T
    lane = lax.broadcasted_iota(jnp.int32, (512, 256), 1).astype(F32)
    for k in range(2):
        for n in range(6):
            hit = cols_t[:, k : k + 1] == lane + 256.0 * n
            comb[n // 3][k * 3 + n % 3] = jnp.where(hit, 1.0, 0.0).astype(BF)
    shares[...] = cols_t
    for i in range(6, 8):
        relay(i)

    def project(e, chip):
        part = at(chip * 1024, 1024, 1024)
        left_side = jnp.concatenate([rows[2 * chip, e], rows[2 * chip + 1, e]], axis=1)
        both = jnp.concatenate([gate_o[e, part, :], up_o[e, part, :]], axis=1)
        return jnp.dot(left_side, both, preferred_element_type=F32)

    def total(e):
        return sd.at[pl.ds(0, 12), :, pl.ds(e * 256, 256)]

    def near(e):
        total(e)[...] = project(e, x).reshape(12, 64, 256)

        def step(j, carry):
            total(e)[...] += project(e, (x + j + j // 2) % 4).reshape(12, 64, 256)
            return carry

        lax.fori_loop(1, 3, step, 0)

    def finish(e):
        last = project(e, (x + 2) % 4) + total(e)[...].reshape(768, 256)
        v = last[:, 0:128]
        hid[t, e] = (v / (1.0 + jnp.exp(-v)) * last[:, 128:256]).astype(BF)

    def hidden_ref(s, e, part):
        return hid.at[s, e] if part is None else hid.at[s, e, pl.ds(part * 384, 384), :]

    def hidden_copy(e, n):
        s, part, who = (
            (t, None, right), (t, None, left), (t, None, mate), (left, None, mate), (left, 0, right),
            (right, None, mate), (right, 1, left), (across, 0, mate), (across, 1, mate),
        )[n]
        ref = hidden_ref(s, e, part)
        slot = {0: 0, 1: 1, 4: 2, 6: 3}.get(n, 4)
        return remote(ref, ref, s_s.at[4], h_r.at[e, slot], f, who)

    half = pl.ds(0, 384)

    for m in range(2):
        arrived(fresh[m].at[0, pl.ds(0, 3840), :], w_r.at[0, m])
    arrived(rows.at[pl.ds(0, 3)], x_b.at[0])
    near(0)
    for i in range(8):
        arrived(rows.at[across, 0, pair, :], x_r.at[i, 2])
        for k in chain[2 * i : 2 * i + 2]:
            row_copy(k, 7).start()
        arrived(rows.at[across, 1, pair, :], x_r.at[i, 3])
        for k in chain[2 * i : 2 * i + 2]:
            row_copy(k, 8).start()
    arrived(rows.at[0], x_b.at[1])
    finish(0)
    for n in range(3):
        hidden_copy(0, n).start()
    for m in range(2):
        arrived(fresh[m].at[1, pl.ds(0, 3840), :], w_r.at[1, m])
    near(1)
    finish(1)
    for n in range(3):
        hidden_copy(1, n).start()

    for e in range(2):
        arrived(hid.at[left, e], h_r.at[e, 0])
        hidden_copy(e, 4).start()
        hidden_copy(e, 3).start()
        arrived(hid.at[right, e], h_r.at[e, 1])
        hidden_copy(e, 6).start()
        hidden_copy(e, 5).start()

    def new_copy(k, e):
        s = (t + k) % 8
        return remote(
            drecv.at[e, at(s * 128, 128, 128), :], down_o.at[e, :, at(t * 512, 512, 512)],
            s_s.at[5], n_r.at[0], f, s,
        )

    def back_copy(k, e):
        return remote(
            stage.at[e * 16 + to(k)], ret[e].at[f], s_s.at[6], b_r.at[e], to(k), t
        )

    for e in range(2):
        for n in range(2):
            arrived(hid.at[across, e, half, :], h_r.at[e, 2 + n])
            hidden_copy(e, 7 + n).start()
        arrived(drecv.at[e, pl.ds(0, 960), :], d_r.at[e])
        arrived(hid.at[pl.ds(0, 4), e], h_r.at[e, 4])

        def expert_out(g, carry):
            part = at(g * 192, 192, 192)
            h = jnp.concatenate([hid[s, e, part, :] for s in range(8)], axis=1)
            out = jnp.dot(h, drecv[e], preferred_element_type=F32).astype(BF)
            stage[pl.ds(e * 16 + g * 4, 4)] = out.reshape(4, CAP, 512)
            return carry

        lax.fori_loop(0, 4, expert_out, 0)
        for k in ORDER:
            back_copy(k, e).start()
        ret[e][f] = stage[e * 16 + f]
        for k in range(1, 8):
            new_copy(k, e).start()
        down_o[e, :, at(t * 512, 512, 512)] = drecv[e, at(t * 128, 128, 128), :]

    arrived(ret0.at[pl.ds(0, 15)], b_r.at[0])
    macc[...] = mix(pf, ret0, shares, pl.ds(0, 512))
    arrived(down_o.at[:, :, pl.ds(0, 3584)], n_r.at[0])
    arrived(ret1.at[pl.ds(0, 15)], b_r.at[1])
    sent(wsend.at[pl.ds(0, 15)], s_s.at[0])
    sent(tsend.at[pl.ds(0, 15)], s_s.at[1])
    sent(rows.at[pl.ds(0, 7)], s_s.at[2])
    sent(dsend.at[pl.ds(0, 15)], s_s.at[3])
    sent(hid.at[pl.ds(0, 7)], s_s.at[4])
    sent(down_o.at[:, :, pl.ds(0, 3584)], s_s.at[5])
    sent(stage.at[pl.ds(0, 30)], s_s.at[6])


def mix(comb, ret, shares, part):
    total = 0.0
    for k in range(2):
        picked = 0.0
        for n in range(3):
            back = ret[...].reshape(768, 512)[n * 256 : (n + 1) * 256]
            picked += jnp.dot(comb[k * 3 + n, part, :], back, preferred_element_type=F32)
        total += picked * shares[part, 2 + k : 3 + k]
    return total


def settle(gate, up, down, ret1, comb1, macc, shares, mixed_o, gate_o, up_o, down_o, mixed, sem):
    moves = [
        pltpu.make_async_copy(src, dst, sem.at[n])
        for n, (src, dst) in enumerate(((gate, gate_o), (up, up_o), (down, down_o)))
    ]
    for move in moves:
        move.start()
    for n in range(4):
        part = pl.ds(n * 128, 128)
        mixed[part, :] = (macc[part, :] + mix(comb1, ret1, shares, part)).astype(BF)
        moves.append(pltpu.make_async_copy(mixed.at[part], mixed_o.at[part], sem.at[3 + n]))
        moves[-1].start()
    for move in moves:
        move.wait()


def on_device(
    prompt, expert_ids, group_weight, expert_share, norm_gain, gate_train, up_train, down_train
):
    any_ref = pl.BlockSpec(memory_space=pl.ANY)
    vmem_ref = pl.BlockSpec(memory_space=pltpu.VMEM)
    hbm_ref = pl.BlockSpec(memory_space=pltpu.HBM)
    dma = pltpu.SemaphoreType.DMA
    made = pl.pallas_call(
        kernel,
        out_shape=(
            jax.ShapeDtypeStruct((2, 4096, 128), BF),
            jax.ShapeDtypeStruct((2, 4096, 128), BF),
            jax.ShapeDtypeStruct((2, 128, 4096), BF),
            jax.ShapeDtypeStruct((16, CAP, 512), BF),
            jax.ShapeDtypeStruct((6, 512, 256), BF),
            jax.ShapeDtypeStruct((512, 512), F32),
            jax.ShapeDtypeStruct((512, 128), F32),
        ),
        in_specs=[hbm_ref] * 8,
        out_specs=(vmem_ref,) * 7,
        scratch_shapes=[
            pltpu.VMEM((2, 512), jnp.int32),
            pltpu.VMEM((1, 512), F32),
            pltpu.VMEM((2, 512), F32),
            pltpu.VMEM((1, 256), F32),
            pltpu.VMEM((16, 512, 256), BF),
            pltpu.VMEM((512, 512), BF),
            pltpu.VMEM((256, 128), F32),
            pltpu.VMEM((16, 2, 256, 128), F32),
            pltpu.VMEM((16, 64, 512), F32),
            pltpu.VMEM((16, 2, 2, 256, 128), BF),
            pltpu.VMEM((16, 2, 64, 512), BF),
            pltpu.VMEM((32, 512), F32),
            pltpu.VMEM((16, 2, CAP, 512), BF),
            pltpu.VMEM((8, 2, 768, 512), BF),
            pltpu.VMEM((2, 1024, 512), BF),
            pltpu.VMEM((8, 2, 768, 128), BF),
            pltpu.VMEM((32, CAP, 512), BF),
            pltpu.VMEM((16, CAP, 512), BF),
            pltpu.VMEM((128, 512), F32),
            dma((4,)), dma((5,)), dma((7,)), dma((16,)), dma((2, 2)), dma((8, 4)), dma((2,)),
            dma((2, 5)), dma((2,)), dma((1,)), dma((2,)),
        ],
        compiler_params=pltpu.CompilerParams(
            collective_id=0, has_side_effects=True, vmem_limit_bytes=45500000
        ),
        name="handover",
    )(
        prompt,
        expert_ids.T,
        group_weight.reshape(1, -1),
        expert_share.T,
        norm_gain.reshape(1, -1),
        gate_train.reshape(16, 2, 256, 128),
        up_train.reshape(16, 2, 256, 128),
        down_train.reshape(16, 2, 64, 512),
    )

    return pl.pallas_call(
        settle,
        out_shape=(
            jax.ShapeDtypeStruct((512, 512), BF),
            jax.ShapeDtypeStruct((2, 4096, 128), BF),
            jax.ShapeDtypeStruct((2, 4096, 128), BF),
            jax.ShapeDtypeStruct((2, 128, 4096), BF),
        ),
        in_specs=[any_ref] * 3 + [vmem_ref] * 4,
        out_specs=(hbm_ref,) * 4,
        scratch_shapes=[pltpu.VMEM((512, 512), BF), dma((7,))],
        compiler_params=pltpu.CompilerParams(vmem_limit_bytes=6 << 20),
        name="settle",
    )(*made)


def solution(mesh):
    placed = (
        P("fs", None),
        P("fs", None),
        P("fs"),
        P("fs", None),
        P("fs"),
        P(None, "fs", "tp"),
        P(None, "fs", "tp"),
        P(None, "fs", "tp"),
    )
    return jax.shard_map(
        on_device,
        mesh=mesh,
        in_specs=placed,
        out_specs=(P("fs", "tp"), P("fs", None, "tp"), P("fs", None, "tp"), P("fs", "tp", None)),
        check_vma=False,
    )
```

time: 132 us -> 122 us (0.924); the launches traced: 132 us -> 120 us
  Pallas kernels: 123 us -> 116 us
  local copies, waits for them, and re-layouts: 8.73 us -> 2.73 us
    pallas_call x1 -> x2, Pallas kernels: 123 us -> 116 us  [the longest x1 114 us: on_device(): pl.pallas_call(kernel, out_shape=(jax.ShapeDtypeStruct((2, 4096, 128), BF...]
    unnamed x8, local copies, waits for them, and re-layouts: 8.73 us -> 2.73 us
where the time goes in v3:
time: 122 us; the launch traced here: 120 us
  Pallas kernels  116 us (95%)
  local copies, waits for them, and re-layouts  2.73 us (2%)
    pallas_call x1, Pallas kernels, on_device(): pl.pallas_call(kernel, out_shape=(jax.ShapeDtypeStruct((2, 4096, 128), BF...  114 us
    pallas_call x1, Pallas kernels, on_device(): pl.pallas_call(settle, out_shape=(jax.ShapeDtypeStruct((512, 512), BF), j...  2.86 us
    unnamed x8, local copies, waits for them, and re-layouts  2.73 us

profile of v3, /device:TPU:1, one launch (start us, length us, event | category | flops | bytes accessed | tf_op | source)
XLA Modules:
  0.0 119.8 jit_solution(18040597493142623376)
XLA Ops:
  0.6 0.0 copy-start
  0.6 0.7 copy-done
  1.3 0.0 copy-start.1
  1.3 0.7 copy-done.1
  2.0 0.0 copy-start.2
  2.0 0.7 copy-done.2
  2.7 0.0 copy-start.3
  2.7 0.7 copy-done.3
  3.4 113.6 %handover.1 = (bf16[2,4096,128]{2,1,0:T(8,128)(2,1)S(1)}, bf16[2,4096,128]{2,1,0:T(8,128)(2,1)S(1)}, bf16[2,128,4096]{2,1,0:T(8,128)(2,1)S(1)}, bf16[16,48,512]{...) custom-call(bf16[512,4096]{1,0:T(8,128)(2,1)} %prompt.1, ...), custom_call_target="tpu_custom_call" | custom-call | tf_op jit(solution)/shard_map/handover/pallas_call | solution.py:420
  117.0 2.9 %settle.1 = (bf16[512,512]{1,0:T(8,128)(2,1)}, bf16[2,4096,128]{2,1,0:T(8,128)(2,1)}, bf16[2,4096,128]{2,1,0:T(8,128)(2,1)}, bf16[2,128,4096]{2,1,0:T(8,128)(2,1)}) custom-call(bf16[2,4096,128]{2,1,0:T(8,128)(2,1)S(1)} %get-tuple-element.11.gate, bf16[2,4096,128]{2,1,0:T(8,128)(2,1)S(1)} %get-tuple-element.12.up, ...), custom_call_target="tpu_custom_call" | custom-call | tf_op jit(solution)/shard_map/settle/pallas_call | solution.py:471
Async XLA Ops:
  0.6 0.7 copy-start
  1.3 0.7 copy-start.1
  2.0 0.7 copy-start.2
  2.7 0.7 copy-start.3

commit v4 on v3

--- a/solution.py
+++ b/solution.py
@@ -14,11 +14,11 @@
 
 
 def kernel(
-    prompt, ids_h, gw_h, share_h, gain_h, gate, up, down,
-    gate_o, up_o, down_o, ret1, comb1, macc, shares,
-    ids, gw, share, gain, pf, xn, gb, sw, sd, wsend, dsend, cm, tsend, rows, drecv,
+    prompt, ids, gain, gate, up, down,
+    gate_o, up_o, down_o, ret1, comb1, picked0,
+    pf, xn, gb, sw, sd, wsend, dsend, cm, tsend, rows, drecv,
     hid, stage, ret0, cols,
-    i_s, l_s, s_s, t_r, w_r, x_r, x_b, h_r, d_r, n_r, b_r,
+    l_s, s_s, t_r, w_r, x_r, x_b, h_r, d_r, n_r, b_r,
 ):
     f = lax.axis_index("fs")
     t = lax.axis_index("tp")
@@ -76,27 +76,19 @@
     def load_weights(i, e, m, sem):
         return local(source[m].at[to(chain[(i + 1) % 16]), e], sw.at[i, m], l_s.at[sem])
 
-    small = [
-        local(src, dst, i_s.at[n])
-        for n, (src, dst) in enumerate(((ids_h, ids), (gw_h, gw), (share_h, share), (gain_h, gain)))
-    ]
-    for load in small:
-        load.start()
+    for i in range(16):
+        local(prompt.at[:, i * 256 : (i + 1) * 256], pf.at[i], l_s.at[1]).start()
     for i in range(8):
         load_weights(i, 0, 0, 0).start()
-    for i in range(16):
-        local(prompt.at[:, i * 256 : (i + 1) * 256], pf.at[i], l_s.at[1]).start()
     for i in range(16):
         for m in range(2):
             if i > 7 or m:
                 load_weights(i, 0, m, 2).start()
 
-    for load in small:
-        load.wait()
     gb[...] = jnp.broadcast_to(gain[...], (128, 256)).T
 
     def rank_slots():
-        expert = lax.broadcasted_iota(jnp.int32, (32, 512), 0)
+        expert = lax.broadcasted_iota(jnp.int32, (32, 512), 0).astype(F32)
         hit0 = ids[0:1, :] == expert
         hit1 = ids[1:2, :] == expert
         named = jnp.where(hit0 | hit1, 1.0, 0.0)
@@ -106,13 +98,12 @@
         ).astype(BF)
         count = jnp.dot(named.astype(BF), before, preferred_element_type=F32)
         cm[...] = jnp.where(named > 0.5, count, -1.0)
-        total = share[0:1, :] + share[1:2, :]
         for k, hit in ((0, hit0), (1, hit1)):
             rank = jnp.sum(jnp.where(hit, count, 0.0), axis=0, keepdims=True)
             expert_of = ids[k : k + 1, :]
-            place = (expert_of & 1) * 768 + (expert_of >> 1) * CAP
-            cols[k : k + 1, :] = place.astype(F32) + rank
-            cols[k + 2 : k + 3, :] = gw[...] * share[k : k + 1, :] / total
+            pair = jnp.floor(expert_of * 0.5)
+            place = (expert_of - 2.0 * pair) * 768.0 + pair * float(CAP)
+            cols[k : k + 1, :] = place + rank
 
     cols[...] = jnp.zeros_like(cols)
     rank_slots()
@@ -132,13 +123,6 @@
             wsend.at[k, e, m], fresh[m].at[e, at(f * 256, 256, 256), :],
             s_s.at[0], w_r.at[e, m], to(k), t,
         )
-
-    local(sw.at[pl.ds(0, 8), 0], sw.at[pl.ds(0, 8), 0], l_s.at[0]).wait()
-    for i in range(8):
-        cast_weights(i, 0, 0)
-    pl.semaphore_wait(barrier, 22)
-    for k in ORDER[:8]:
-        weights_copy(k, 0, 0).start()
 
     local(pf, pf, l_s.at[1]).wait()
 
@@ -169,10 +153,16 @@
             s_s.at[1], t_r.at[k], to(k), t,
         )
 
+    pl.semaphore_wait(barrier, 22)
     for k in ORDER:
         token_copy(k).start()
     rows[t, :, at(f * CAP, CAP, CAP), :] = tsend[f]
 
+    local(sw.at[pl.ds(0, 8), 0], sw.at[pl.ds(0, 8), 0], l_s.at[0]).wait()
+    for i in range(8):
+        cast_weights(i, 0, 0)
+    for k in ORDER[:8]:
+        weights_copy(k, 0, 0).start()
     local(sw.at[pl.ds(0, 12)], sw.at[pl.ds(0, 12)], l_s.at[2]).wait()
     for m in range(2):
         for i in range(16):
@@ -265,7 +255,6 @@
         for n in range(6):
             hit = cols_t[:, k : k + 1] == lane + 256.0 * n
             comb[n // 3][k * 3 + n % 3] = jnp.where(hit, 1.0, 0.0).astype(BF)
-    shares[...] = cols_t
     for i in range(6, 8):
         relay(i)
 
@@ -337,7 +326,7 @@
         hidden_copy(e, 5).start()
 
     def new_copy(k, e):
-        s = (t + k) % 8
+        s = (x + k // 2) % 4 * 2 + (c + k) % 2
         return remote(
             drecv.at[e, at(s * 128, 128, 128), :], down_o.at[e, :, at(t * 512, 512, 512)],
             s_s.at[5], n_r.at[0], f, s,
@@ -353,6 +342,8 @@
             arrived(hid.at[across, e, half, :], h_r.at[e, 2 + n])
             hidden_copy(e, 7 + n).start()
         arrived(drecv.at[e, pl.ds(0, 960), :], d_r.at[e])
+        for k in (2, 6, 3, 7, 4, 5, 1):
+            new_copy(k, e).start()
         arrived(hid.at[pl.ds(0, 4), e], h_r.at[e, 4])
 
         def expert_out(g, carry):
@@ -366,12 +357,11 @@
         for k in ORDER:
             back_copy(k, e).start()
         ret[e][f] = stage[e * 16 + f]
-        for k in range(1, 8):
-            new_copy(k, e).start()
         down_o[e, :, at(t * 512, 512, 512)] = drecv[e, at(t * 128, 128, 128), :]
 
     arrived(ret0.at[pl.ds(0, 15)], b_r.at[0])
-    macc[...] = mix(pf, ret0, shares, pl.ds(0, 512))
+    for k in range(2):
+        picked0[k] = pick_rows(pf, ret0, k, pl.ds(0, 512)).astype(BF)
     arrived(down_o.at[:, :, pl.ds(0, 3584)], n_r.at[0])
     arrived(ret1.at[pl.ds(0, 15)], b_r.at[1])
     sent(wsend.at[pl.ds(0, 15)], s_s.at[0])
@@ -383,27 +373,35 @@
     sent(stage.at[pl.ds(0, 30)], s_s.at[6])
 
 
-def mix(comb, ret, shares, part):
-    total = 0.0
-    for k in range(2):
-        picked = 0.0
-        for n in range(3):
-            back = ret[...].reshape(768, 512)[n * 256 : (n + 1) * 256]
-            picked += jnp.dot(comb[k * 3 + n, part, :], back, preferred_element_type=F32)
-        total += picked * shares[part, 2 + k : 3 + k]
-    return total
-
-
-def settle(gate, up, down, ret1, comb1, macc, shares, mixed_o, gate_o, up_o, down_o, mixed, sem):
+def pick_rows(comb, ret, k, part):
+    picked = 0.0
+    for n in range(3):
+        back = ret[...].reshape(768, 512)[n * 256 : (n + 1) * 256]
+        picked += jnp.dot(comb[k * 3 + n, part, :], back, preferred_element_type=F32)
+    return picked
+
+
+def settle(
+    gate, up, down, ret1, comb1, picked0, gw, share,
+    mixed_o, gate_o, up_o, down_o, mixed, weight, sem,
+):
     moves = [
         pltpu.make_async_copy(src, dst, sem.at[n])
         for n, (src, dst) in enumerate(((gate, gate_o), (up, up_o), (down, down_o)))
     ]
     for move in moves:
         move.start()
+    total = share[0:1, :] + share[1:2, :]
+    for k in range(2):
+        row = gw[...] * share[k : k + 1, :] / total
+        weight[k] = jnp.broadcast_to(row, (128, 512)).T
     for n in range(4):
         part = pl.ds(n * 128, 128)
-        mixed[part, :] = (macc[part, :] + mix(comb1, ret1, shares, part)).astype(BF)
+        sums = []
+        for k in range(2):
+            value = picked0[k, part, :].astype(F32) + pick_rows(comb1, ret1, k, part)
+            sums.append(value * weight[k, part, 0:1])
+        mixed[part, :] = (sums[0] + sums[1]).astype(BF)
         moves.append(pltpu.make_async_copy(mixed.at[part], mixed_o.at[part], sem.at[3 + n]))
         moves[-1].start()
     for move in moves:
@@ -425,16 +423,11 @@
             jax.ShapeDtypeStruct((2, 128, 4096), BF),
             jax.ShapeDtypeStruct((16, CAP, 512), BF),
             jax.ShapeDtypeStruct((6, 512, 256), BF),
-            jax.ShapeDtypeStruct((512, 512), F32),
-            jax.ShapeDtypeStruct((512, 128), F32),
+            jax.ShapeDtypeStruct((2, 512, 512), BF),
         ),
-        in_specs=[hbm_ref] * 8,
-        out_specs=(vmem_ref,) * 7,
+        in_specs=[hbm_ref, vmem_ref, vmem_ref] + [hbm_ref] * 3,
+        out_specs=(vmem_ref,) * 6,
         scratch_shapes=[
-            pltpu.VMEM((2, 512), jnp.int32),
-            pltpu.VMEM((1, 512), F32),
-            pltpu.VMEM((2, 512), F32),
-            pltpu.VMEM((1, 256), F32),
             pltpu.VMEM((16, 512, 256), BF),
             pltpu.VMEM((512, 512), BF),
             pltpu.VMEM((256, 128), F32),
@@ -450,18 +443,16 @@
             pltpu.VMEM((32, CAP, 512), BF),
             pltpu.VMEM((16, CAP, 512), BF),
             pltpu.VMEM((128, 512), F32),
-            dma((4,)), dma((5,)), dma((7,)), dma((16,)), dma((2, 2)), dma((8, 4)), dma((2,)),
+            dma((5,)), dma((7,)), dma((16,)), dma((2, 2)), dma((8, 4)), dma((2,)),
             dma((2, 5)), dma((2,)), dma((1,)), dma((2,)),
         ],
         compiler_params=pltpu.CompilerParams(
-            collective_id=0, has_side_effects=True, vmem_limit_bytes=45500000
+            collective_id=0, has_side_effects=True, vmem_limit_bytes=46000000
         ),
         name="handover",
     )(
         prompt,
-        expert_ids.T,
-        group_weight.reshape(1, -1),
-        expert_share.T,
+        expert_ids.T.astype(F32),
         norm_gain.reshape(1, -1),
         gate_train.reshape(16, 2, 256, 128),
         up_train.reshape(16, 2, 256, 128),
@@ -476,12 +467,12 @@
             jax.ShapeDtypeStruct((2, 4096, 128), BF),
             jax.ShapeDtypeStruct((2, 128, 4096), BF),
         ),
-        in_specs=[any_ref] * 3 + [vmem_ref] * 4,
+        in_specs=[any_ref] * 3 + [vmem_ref] * 5,
         out_specs=(hbm_ref,) * 4,
-        scratch_shapes=[pltpu.VMEM((512, 512), BF), dma((7,))],
+        scratch_shapes=[pltpu.VMEM((512, 512), BF), pltpu.VMEM((2, 512, 128), F32), dma((7,))],
         compiler_params=pltpu.CompilerParams(vmem_limit_bytes=6 << 20),
         name="settle",
-    )(*made)
+    )(*made, group_weight.reshape(1, -1), expert_share.T)
 
 
 def solution(mesh):

time: 122 us -> 118 us (0.967)
  local copies, waits for them, and re-layouts: 2.73 us -> 0.69 us
    unnamed x8 -> x6, local copies, waits for them, and re-layouts: 2.73 us -> 0.69 us
    pallas_call x1, Pallas kernels: 114 us -> 112 us  [on_device(): pl.pallas_call(kernel, out_shape=(jax.ShapeDtypeStruct((2, 4096, 128), BF...]
where the time goes in v4:
time: 118 us; the launch traced here: 117 us
  Pallas kernels  115 us (97%)
    pallas_call x1, Pallas kernels, on_device(): pl.pallas_call(kernel, out_shape=(jax.ShapeDtypeStruct((2, 4096, 128), BF...  112 us
    pallas_call x1, Pallas kernels, on_device(): pl.pallas_call(settle, out_shape=(jax.ShapeDtypeStruct((512, 512), BF), j...  2.86 us

profile of v4, /device:TPU:1, one launch (start us, length us, event | category | flops | bytes accessed | tf_op | source)
XLA Modules:
  0.0 117.0 jit_solution(13358260623709947260)
XLA Ops:
  0.6 0.7 convert_bitcast_fusion.ids
  1.3 0.0 copy-start.2
  1.3 0.7 copy-done.2
  2.0 0.0 copy-start
  2.0 0.0 copy-start.1
  2.0 112.1 %handover.1 = (bf16[2,4096,128]{2,1,0:T(8,128)(2,1)S(1)}, bf16[2,4096,128]{2,1,0:T(8,128)(2,1)S(1)}, bf16[2,128,4096]{2,1,0:T(8,128)(2,1)S(1)}, bf16[16,48,512]{...) custom-call(bf16[512,4096]{1,0:T(8,128)(2,1)} %prompt.1, ...), custom_call_target="tpu_custom_call" | custom-call | tf_op jit(solution)/shard_map/handover/pallas_call | solution.py:418
  114.1 0.0 copy-done
  114.1 0.0 copy-done.1
  114.1 2.9 %settle.1 = (bf16[512,512]{1,0:T(8,128)(2,1)}, bf16[2,4096,128]{2,1,0:T(8,128)(2,1)}, bf16[2,4096,128]{2,1,0:T(8,128)(2,1)}, bf16[2,128,4096]{2,1,0:T(8,128)(2,1)}) custom-call(bf16[2,4096,128]{2,1,0:T(8,128)(2,1)S(1)} %get-tuple-element.10.gate, bf16[2,4096,128]{2,1,0:T(8,128)(2,1)S(1)} %get-tuple-element.11.up, ...), custom_call_target="tpu_custom_call" | custom-call | tf_op jit(solution)/shard_map/settle/pallas_call | solution.py:462
Async XLA Ops:
  1.3 0.7 copy-start.2
  2.0 112.1 %copy-start = (f32[512,2]{0,1:T(2,128)S(1)}, f32[512,2]{0,1:T(2,128)}, u32[]{:S(2)}) copy-start(f32[512,2]{0,1:T(2,128)} %param.11) | copy-start | bytes 12292
  2.0 112.1 %copy-start.1 = (f32[512]{0:T(512)S(1)}, f32[512]{0:T(512)}, u32[]{:S(2)}) copy-start(f32[512]{0:T(512)} %param.10) | copy-start | bytes 6148

commit v5 on v4

--- a/solution.py
+++ b/solution.py
@@ -14,7 +14,7 @@
 
 
 def kernel(
-    prompt, ids, gain, gate, up, down,
+    prompt, small, gate, up, down,
     gate_o, up_o, down_o, ret1, comb1, picked0,
     pf, xn, gb, sw, sd, wsend, dsend, cm, tsend, rows, drecv,
     hid, stage, ret0, cols,
@@ -67,6 +67,13 @@
     lax.fori_loop(1, 16, greet_fs, 0)
     lax.fori_loop(1, 8, greet_tp, 0)
 
+    for half_rows in range(2):
+        block = pl.ds(half_rows * 256, 256)
+        for i in range(16):
+            local(
+                prompt.at[block, i * 256 : (i + 1) * 256], pf.at[i, block, :], l_s.at[half_rows]
+            ).start()
+
     chain = (0,) + ORDER
     source = (gate, up)
     fresh = (gate_o, up_o)
@@ -76,16 +83,15 @@
     def load_weights(i, e, m, sem):
         return local(source[m].at[to(chain[(i + 1) % 16]), e], sw.at[i, m], l_s.at[sem])
 
-    for i in range(16):
-        local(prompt.at[:, i * 256 : (i + 1) * 256], pf.at[i], l_s.at[1]).start()
     for i in range(8):
-        load_weights(i, 0, 0, 0).start()
+        load_weights(i, 0, 0, 5).start()
     for i in range(16):
         for m in range(2):
             if i > 7 or m:
                 load_weights(i, 0, m, 2).start()
 
-    gb[...] = jnp.broadcast_to(gain[...], (128, 256)).T
+    ids = small.at[0:2]
+    gb[...] = jnp.broadcast_to(small[2:3, 0:256], (128, 256)).T
 
     def rank_slots():
         expert = lax.broadcasted_iota(jnp.int32, (32, 512), 0).astype(F32)
@@ -124,8 +130,6 @@
             s_s.at[0], w_r.at[e, m], to(k), t,
         )
 
-    local(pf, pf, l_s.at[1]).wait()
-
     def normalize(i, carry):
         block = at(i * 32, 32, 32)
         squares = jnp.zeros((32, 256), F32)
@@ -139,7 +143,10 @@
             xn[block, h * 256 : (h + 1) * 256] = (part * scale).astype(BF)
         return carry
 
-    lax.fori_loop(0, 16, normalize, 0, unroll=4)
+    for half_rows in range(2):
+        ready = pf.at[:, pl.ds(half_rows * 256, 256), :]
+        local(ready, ready, l_s.at[half_rows]).wait()
+        lax.fori_loop(half_rows * 8, half_rows * 8 + 8, normalize, 0, unroll=4)
 
     for g in range(4):
         chosen = stage[g * 8 : g * 8 + 8].reshape(384, 512)
@@ -147,18 +154,20 @@
             jnp.dot(chosen, xn[...], preferred_element_type=F32).astype(BF).reshape(4, 2, CAP, 512)
         )
 
-    def token_copy(k):
+    def token_copy(k, e):
         return remote(
-            tsend.at[to(k)], rows.at[t, :, at(f * CAP, CAP, CAP), :],
+            tsend.at[to(k), e], rows.at[t, e, at(f * CAP, CAP, CAP), :],
             s_s.at[1], t_r.at[k], to(k), t,
         )
 
     pl.semaphore_wait(barrier, 22)
-    for k in ORDER:
-        token_copy(k).start()
+    for near in (ORDER[:4], ORDER[4:8], ORDER[8:11], ORDER[11:]):
+        for e in range(2):
+            for k in near:
+                token_copy(k, e).start()
     rows[t, :, at(f * CAP, CAP, CAP), :] = tsend[f]
 
-    local(sw.at[pl.ds(0, 8), 0], sw.at[pl.ds(0, 8), 0], l_s.at[0]).wait()
+    local(sw.at[pl.ds(0, 8), 0], sw.at[pl.ds(0, 8), 0], l_s.at[5]).wait()
     for i in range(8):
         cast_weights(i, 0, 0)
     for k in ORDER[:8]:
@@ -415,6 +424,9 @@
     vmem_ref = pl.BlockSpec(memory_space=pltpu.VMEM)
     hbm_ref = pl.BlockSpec(memory_space=pltpu.HBM)
     dma = pltpu.SemaphoreType.DMA
+    packed = lax.pad(expert_ids, 0, ((0, 0, 0), (0, 6, 0))).astype(F32) + lax.pad(
+        norm_gain[:, None], 0.0, ((0, 256, 0), (2, 5, 0))
+    )
     made = pl.pallas_call(
         kernel,
         out_shape=(
@@ -425,7 +437,7 @@
             jax.ShapeDtypeStruct((6, 512, 256), BF),
             jax.ShapeDtypeStruct((2, 512, 512), BF),
         ),
-        in_specs=[hbm_ref, vmem_ref, vmem_ref] + [hbm_ref] * 3,
+        in_specs=[hbm_ref, vmem_ref] + [hbm_ref] * 3,
         out_specs=(vmem_ref,) * 6,
         scratch_shapes=[
             pltpu.VMEM((16, 512, 256), BF),
@@ -443,7 +455,7 @@
             pltpu.VMEM((32, CAP, 512), BF),
             pltpu.VMEM((16, CAP, 512), BF),
             pltpu.VMEM((128, 512), F32),
-            dma((5,)), dma((7,)), dma((16,)), dma((2, 2)), dma((8, 4)), dma((2,)),
+            dma((6,)), dma((7,)), dma((16,)), dma((2, 2)), dma((8, 4)), dma((2,)),
             dma((2, 5)), dma((2,)), dma((1,)), dma((2,)),
         ],
         compiler_params=pltpu.CompilerParams(
@@ -452,8 +464,7 @@
         name="handover",
     )(
         prompt,
-        expert_ids.T.astype(F32),
-        norm_gain.reshape(1, -1),
+        packed.T,
         gate_train.reshape(16, 2, 256, 128),
         up_train.reshape(16, 2, 256, 128),
         down_train.reshape(16, 2, 64, 512),

time: 118 us -> 117 us (level)
  no operation moved by 1% of the time
where the time goes in v5:
time: 117 us; the launch traced here: 116 us
  Pallas kernels  115 us (98%)
    pallas_call x1, Pallas kernels, on_device(): pl.pallas_call(kernel, out_shape=(jax.ShapeDtypeStruct((2, 4096, 128), BF...  112 us
    pallas_call x1, Pallas kernels, on_device(): pl.pallas_call(settle, out_shape=(jax.ShapeDtypeStruct((512, 512), BF), j...  2.86 us

profile of v5, /device:TPU:1, one launch (start us, length us, event | category | flops | bytes accessed | tf_op | source)
XLA Modules:
  0.0 116.3 jit_solution(556169275903135023)
XLA Ops:
  0.6 0.7 add_bitcast_fusion.small
  1.3 0.0 copy-start
  1.3 0.0 copy-start.1
  1.4 112.1 %handover.1 = (bf16[2,4096,128]{2,1,0:T(8,128)(2,1)S(1)}, bf16[2,4096,128]{2,1,0:T(8,128)(2,1)S(1)}, bf16[2,128,4096]{2,1,0:T(8,128)(2,1)S(1)}, bf16[16,48,512]{...) custom-call(bf16[512,4096]{1,0:T(8,128)(2,1)} %prompt.1, ...), custom_call_target="tpu_custom_call" | custom-call | tf_op jit(solution)/shard_map/handover/pallas_call | solution.py:430
  113.4 0.0 copy-done
  113.4 0.0 copy-done.1
  113.5 2.9 %settle.1 = (bf16[512,512]{1,0:T(8,128)(2,1)}, bf16[2,4096,128]{2,1,0:T(8,128)(2,1)}, bf16[2,4096,128]{2,1,0:T(8,128)(2,1)}, bf16[2,128,4096]{2,1,0:T(8,128)(2,1)}) custom-call(bf16[2,4096,128]{2,1,0:T(8,128)(2,1)S(1)} %get-tuple-element.10.gate, bf16[2,4096,128]{2,1,0:T(8,128)(2,1)S(1)} %get-tuple-element.11.up, ...), custom_call_target="tpu_custom_call" | custom-call | tf_op jit(solution)/shard_map/settle/pallas_call | solution.py:473
Async XLA Ops:
  1.3 112.1 %copy-start = (f32[512,2]{0,1:T(2,128)S(1)}, f32[512,2]{0,1:T(2,128)}, u32[]{:S(2)}) copy-start(f32[512,2]{0,1:T(2,128)} %param.11) | copy-start | bytes 12292
  1.3 112.1 %copy-start.1 = (f32[512]{0:T(512)S(1)}, f32[512]{0:T(512)}, u32[]{:S(2)}) copy-start(f32[512]{0:T(512)} %param.10) | copy-start | bytes 6148

commit v6 on v5

--- a/solution.py
+++ b/solution.py
@@ -16,7 +16,7 @@
 def kernel(
     prompt, small, gate, up, down,
     gate_o, up_o, down_o, ret1, comb1, picked0,
-    pf, xn, gb, sw, sd, wsend, dsend, cm, tsend, rows, drecv,
+    pf, po, xn, gb, sw, sd, wsend, dsend, cm, tsend, rows, drecv,
     hid, stage, ret0, cols,
     l_s, s_s, t_r, w_r, x_r, x_b, h_r, d_r, n_r, b_r,
 ):
@@ -54,6 +54,11 @@
     def sent(ref, sem):
         remote(ref, ref, sem, n_r.at[0], f, mate).wait_send()
 
+    local(prompt.at[:, at(t * 512, 512, 512)], po, l_s.at[0]).start()
+    for i in range(4):
+        block = pl.ds(i * 128, 128)
+        local(prompt.at[block, :], pf.at[block, :], l_s.at[i // 2]).start()
+
     barrier = pltpu.get_barrier_semaphore()
 
     def greet_fs(k, carry):
@@ -66,19 +71,11 @@
 
     lax.fori_loop(1, 16, greet_fs, 0)
     lax.fori_loop(1, 8, greet_tp, 0)
-
-    for half_rows in range(2):
-        block = pl.ds(half_rows * 256, 256)
-        for i in range(16):
-            local(
-                prompt.at[block, i * 256 : (i + 1) * 256], pf.at[i, block, :], l_s.at[half_rows]
-            ).start()
 
     chain = (0,) + ORDER
     source = (gate, up)
     fresh = (gate_o, up_o)
     ret = (ret0, ret1)
-    comb = (pf, comb1)
 
     def load_weights(i, e, m, sem):
         return local(source[m].at[to(chain[(i + 1) % 16]), e], sw.at[i, m], l_s.at[sem])
@@ -134,17 +131,14 @@
         block = at(i * 32, 32, 32)
         squares = jnp.zeros((32, 256), F32)
         for j in range(16):
-            part = pf[j, block, :].astype(F32)
+            part = pf[block, j * 256 : (j + 1) * 256].astype(F32)
             squares = squares + part * part
         mean = jnp.sum(squares, axis=1, keepdims=True) * (1.0 / 4096.0)
-        scale = lax.rsqrt(mean + EPS)
-        for h in range(2):
-            part = pf[2 * t + h, block, :].astype(F32)
-            xn[block, h * 256 : (h + 1) * 256] = (part * scale).astype(BF)
+        xn[block, :] = (po[block, :].astype(F32) * lax.rsqrt(mean + EPS)).astype(BF)
         return carry
 
-    for half_rows in range(2):
-        ready = pf.at[:, pl.ds(half_rows * 256, 256), :]
+    for half_rows, size in ((0, 320), (1, 256)):
+        ready = pf.at[pl.ds(0, size), :]
         local(ready, ready, l_s.at[half_rows]).wait()
         lax.fori_loop(half_rows * 8, half_rows * 8 + 8, normalize, 0, unroll=4)
 
@@ -263,7 +257,11 @@
     for k in range(2):
         for n in range(6):
             hit = cols_t[:, k : k + 1] == lane + 256.0 * n
-            comb[n // 3][k * 3 + n % 3] = jnp.where(hit, 1.0, 0.0).astype(BF)
+            chosen = jnp.where(hit, 1.0, 0.0).astype(BF)
+            if n < 3:
+                pf[:, (k * 3 + n) * 256 : (k * 3 + n + 1) * 256] = chosen
+            else:
+                comb1[k * 3 + n - 3] = chosen
     for i in range(6, 8):
         relay(i)
 
@@ -370,7 +368,8 @@
 
     arrived(ret0.at[pl.ds(0, 15)], b_r.at[0])
     for k in range(2):
-        picked0[k] = pick_rows(pf, ret0, k, pl.ds(0, 512)).astype(BF)
+        blocks = [pf[:, (k * 3 + n) * 256 : (k * 3 + n + 1) * 256] for n in range(3)]
+        picked0[k] = pick_rows(blocks, ret0).astype(BF)
     arrived(down_o.at[:, :, pl.ds(0, 3584)], n_r.at[0])
     arrived(ret1.at[pl.ds(0, 15)], b_r.at[1])
     sent(wsend.at[pl.ds(0, 15)], s_s.at[0])
@@ -382,11 +381,11 @@
     sent(stage.at[pl.ds(0, 30)], s_s.at[6])
 
 
-def pick_rows(comb, ret, k, part):
+def pick_rows(blocks, ret):
     picked = 0.0
     for n in range(3):
         back = ret[...].reshape(768, 512)[n * 256 : (n + 1) * 256]
-        picked += jnp.dot(comb[k * 3 + n, part, :], back, preferred_element_type=F32)
+        picked += jnp.dot(blocks[n], back, preferred_element_type=F32)
     return picked
 
 
@@ -408,7 +407,8 @@
         part = pl.ds(n * 128, 128)
         sums = []
         for k in range(2):
-            value = picked0[k, part, :].astype(F32) + pick_rows(comb1, ret1, k, part)
+            blocks = [comb1[k * 3 + m, part, :] for m in range(3)]
+            value = picked0[k, part, :].astype(F32) + pick_rows(blocks, ret1)
             sums.append(value * weight[k, part, 0:1])
         mixed[part, :] = (sums[0] + sums[1]).astype(BF)
         moves.append(pltpu.make_async_copy(mixed.at[part], mixed_o.at[part], sem.at[3 + n]))
@@ -440,7 +440,8 @@
         in_specs=[hbm_ref, vmem_ref] + [hbm_ref] * 3,
         out_specs=(vmem_ref,) * 6,
         scratch_shapes=[
-            pltpu.VMEM((16, 512, 256), BF),
+            pltpu.VMEM((512, 4096), BF),
+            pltpu.VMEM((512, 512), BF),
             pltpu.VMEM((512, 512), BF),
             pltpu.VMEM((256, 128), F32),
             pltpu.VMEM((16, 2, 256, 128), F32),

time: 117 us -> 117 us (level)
  no operation moved by 1% of the time
where the time goes in v6:
time: 117 us; the launch traced here: 116 us
  Pallas kernels  115 us (98%)
    pallas_call x1, Pallas kernels, on_device(): pl.pallas_call(kernel, out_shape=(jax.ShapeDtypeStruct((2, 4096, 128), BF...  112 us
    pallas_call x1, Pallas kernels, on_device(): pl.pallas_call(settle, out_shape=(jax.ShapeDtypeStruct((512, 512), BF), j...  2.86 us

profile of v6, /device:TPU:1, one launch (start us, length us, event | category | flops | bytes accessed | tf_op | source)
XLA Modules:
  0.0 116.2 jit_solution(2219203362295915852)
XLA Ops:
  0.6 0.7 add_bitcast_fusion.small
  1.3 0.0 copy-start
  1.3 0.0 copy-start.1
  1.4 111.9 %handover.1 = (bf16[2,4096,128]{2,1,0:T(8,128)(2,1)S(1)}, bf16[2,4096,128]{2,1,0:T(8,128)(2,1)S(1)}, bf16[2,128,4096]{2,1,0:T(8,128)(2,1)S(1)}, bf16[16,48,512]{...) custom-call(bf16[512,4096]{1,0:T(8,128)(2,1)} %prompt.1, ...), custom_call_target="tpu_custom_call" | custom-call | tf_op jit(solution)/shard_map/handover/pallas_call | solution.py:430
  113.3 0.0 copy-done
  113.3 0.0 copy-done.1
  113.3 2.9 %settle.1 = (bf16[512,512]{1,0:T(8,128)(2,1)}, bf16[2,4096,128]{2,1,0:T(8,128)(2,1)}, bf16[2,4096,128]{2,1,0:T(8,128)(2,1)}, bf16[2,128,4096]{2,1,0:T(8,128)(2,1)}) custom-call(bf16[2,4096,128]{2,1,0:T(8,128)(2,1)S(1)} %get-tuple-element.10.gate, bf16[2,4096,128]{2,1,0:T(8,128)(2,1)S(1)} %get-tuple-element.11.up, ...), custom_call_target="tpu_custom_call" | custom-call | tf_op jit(solution)/shard_map/settle/pallas_call | solution.py:474
Async XLA Ops:
  1.3 112.0 %copy-start = (f32[512,2]{0,1:T(2,128)S(1)}, f32[512,2]{0,1:T(2,128)}, u32[]{:S(2)}) copy-start(f32[512,2]{0,1:T(2,128)} %param.11) | copy-start | bytes 12292
  1.3 112.0 %copy-start.1 = (f32[512]{0:T(512)S(1)}, f32[512]{0:T(512)}, u32[]{:S(2)}) copy-start(f32[512]{0:T(512)} %param.10) | copy-start | bytes 6148
